TPU v7x, 32 devices: a whole 2x2x4 slice. The times are simulated.
32 devices in a mesh: gr: 2 (over x), fs: 4 (over z), tp: 4 (over y, core).
Axes of the slice: x: 2, y: 2, z: 4, core: 2. Of those that a mesh axis runs over, the one named last changes fastest.
Arguments:
- prompt_tokens: bfloat16 [4096, 2048], P(('gr', 'fs', 'tp')), may hold values from -60 to 60
- norm_gain: float32 [2048], P(('gr', 'fs')), may hold values from 0.1 to 1.9
- up_master: float32 [2048, 8192], P(('gr', 'fs'), 'tp'), may hold values from -0.125 to 0.125
- down_master: float32 [2048, 8192], P(('gr', 'fs'), 'tp'), may hold values from -0.0625 to 0.0625
Outputs:
- up_served: bfloat16 [2048, 8192], P(None, 'tp')
- down_served: bfloat16 [2048, 8192], P(None, 'tp')
- mlp_output: bfloat16 [4096, 2048], P(('gr', 'fs', 'tp'))
All inputs are finite; a program needn't handle non-finite values.
Results may differ from a plain program's by a relative error of at most 0.014.
Values may be sent and summed in bfloat16 or wider, within the bound.
A program may use at most 128 MiB of HBM per device.

v0:
```python
import functools

import jax
import jax.numpy as jnp
from jax import lax
from jax.experimental import pallas as pl
from jax.experimental.pallas import tpu as pltpu
from jax.sharding import PartitionSpec as P

MESH = pl.DeviceIdType.MESH
CHUNK_BYTES = 256 * 1024


def pieces_of(rows, most):
    count = max(1, -(-rows // most))
    units = rows // 16
    cuts = [16 * (units * i // count) for i in range(count + 1)]
    return [(a, b - a) for a, b in zip(cuts, cuts[1:])]


def kernel(
    sizes, tok_hbm, gain_ref, up_hbm, down_hbm,
    up_ref, down_ref, out_ref,
    tok_ref, stage, normed, hidden, part, arrived,
    load_sem, tok_send, tok_recv,
    z_recv, right_send, left_send, x_recv, x_send, part_send, part_recv,
):
    n_gr, n_fs, n_tp = sizes
    g, z, t = lax.axis_index("gr"), lax.axis_index("fs"), lax.axis_index("tp")
    rows, width = stage.shape[1:]
    local = tok_ref.shape[0]
    depth = up_ref.shape[0]
    last = n_fs - 1
    has_right, has_left = z < last, z > 0
    masters = (up_ref, down_ref)

    def crossing(numerator):
        return max(16, rows * numerator // 256 * 16)

    most = max(16, CHUNK_BYTES // (2 * width) // 16 * 16)
    x_first = (crossing(3), crossing(3))
    tables = []
    for p in range(2):
        table = pieces_of(rows - x_first[p], most)
        tables.append(table + [(rows - x_first[p], x_first[p])] * 2)

    def at(p, col, zz, k):
        start, size = tables[p][k]
        base = pl.multiple_of((col * n_fs + zz) * rows, rows)
        return masters[p].at[pl.ds(pl.multiple_of(base + start, 16), size), :]

    def count(p):
        return len(tables[p]) - 2

    def z_copy(p, zz, k, right):
        col = 1 - g if k == count(p) + 1 else g
        ref = at(p, col, zz, k)
        send = right_send if right else left_send
        return pltpu.make_async_remote_copy(
            src_ref=ref, dst_ref=ref, send_sem=send.at[p, zz, k], recv_sem=z_recv.at[p, zz, k],
            device_id=(g, jnp.where(has_right, z + 1, z - 1) if right else jnp.where(has_left, z - 1, z + 1), t),
            device_id_type=MESH,
        )

    def x_copy(p, zz, k, col):
        ref = at(p, col, zz, k)
        return pltpu.make_async_remote_copy(
            src_ref=ref, dst_ref=ref, send_sem=x_send.at[p, zz, k], recv_sem=x_recv.at[p, zz, k],
            device_id=(1 - g, z, t), device_id_type=MESH,
        )

    def send_both(p, k):
        pl.when(has_right)(lambda: z_copy(p, z, k, True).start())
        pl.when(has_left)(lambda: z_copy(p, z, k, False).start())

    def own_z(p):
        for k in range(count(p) + 1):
            send_both(p, k)

    def own_x(p):
        x_copy(p, z, count(p), g).start()
        for k in range(count(p)):
            x_copy(p, z, k, g).start()

    def other_xz(p):
        x_copy(p, z, count(p), 1 - g).wait_recv()
        send_both(p, count(p) + 1)

    def slot(p, s, items=None):
        from_left, from_right = z - s >= 0, z + s <= last
        for k in range(count(p) + 2) if items is None else items:
            def left_in():
                z_copy(p, z - s, k, True).wait_recv()
                if s < last:
                    pl.when(has_right)(lambda: z_copy(p, z - s, k, True).start())
                if k < count(p):
                    x_copy(p, z - s, k, g).start()

            def right_in():
                z_copy(p, z + s, k, False).wait_recv()
                if s < last:
                    pl.when(has_left)(lambda: z_copy(p, z + s, k, False).start())
                if k < count(p):
                    x_copy(p, z + s, k, g).start()

            pl.when(from_left)(left_in)
            pl.when(from_right)(right_in)

    def token_copy(j):
        mine = normed.at[pl.ds(pl.multiple_of(t * local, local), local), :]
        return pltpu.make_async_remote_copy(
            src_ref=mine, dst_ref=mine, send_sem=tok_send.at[j - 1], recv_sem=tok_recv.at[j - 1],
            device_id=(g, z, lax.rem(t + j, n_tp)), device_id_type=MESH,
        )

    far = jnp.where(z + z >= last, 0, last)
    splits = (0, count(1) * 4 // 7, count(1) * 6 // 7, count(1))
    starts = [tables[1][k][0] for k in splits[:3]] + [rows]
    shares = [(a, b - a) for a, b in zip(starts, starts[1:])]
    whole_block = (0, rows)

    def part_copy(block, share, i, j):
        to = lax.rem(t + j, n_tp)
        start, size = share
        base = pl.multiple_of(block * rows, rows)
        row = pl.ds(pl.multiple_of(base + start, 16), size)
        return pltpu.make_async_remote_copy(
            src_ref=part.at[row, pl.ds(pl.multiple_of(to * local, local), local)],
            dst_ref=arrived.at[j - 1, row, :],
            send_sem=part_send.at[block, i, j - 1], recv_sem=part_recv.at[block, i, j - 1],
            device_id=(g, z, to), device_id_type=MESH,
        )

    def multiply(block, share, i):
        start, size = share
        base = pl.multiple_of(block * rows, rows)
        row = pl.ds(pl.multiple_of(base + start, 16), size)
        part[row, :] = lax.dot_general(
            down_ref[row, :], hidden[...], (((1,), (1,)), ((), ())),
            preferred_element_type=jnp.float32,
        ).astype(part.dtype)
        for j in range(1, n_tp):
            part_copy(block, share, i, j).start()

    def second(s):
        def one(i, carry):
            other, side = i // 2, lax.rem(i, 2)
            dist = s - other
            zz = z + (2 * side - 1) * dist
            ok = (dist >= 0) & (zz >= 0) & (zz <= last) & ((dist > 0) | (side == 0)) & (zz != far)

            @pl.when(ok)
            def _():
                @pl.when(other == 1)
                def _():
                    for k in range(count(1)):
                        x_copy(1, zz, k, 1 - g).wait_recv()

                multiply(jnp.where(other == 1, 1 - g, g) * n_fs + zz, whole_block, 0)

            return carry

        lax.fori_loop(0, 4, one, 0)

    def far_share(col, i):
        if shares[i][1] > 0:
            multiply(col * n_fs + far, shares[i], i)

    def far_x(i):
        for k in range(splits[i], splits[i + 1]):
            x_copy(1, far, k, 1 - g).wait_recv()

    def far_blocks():
        slot(1, last, range(splits[0], splits[1]))
        second(last)
        far_share(g, 0)
        slot(1, last, range(splits[1], splits[2]))
        far_x(0)
        far_share(1 - g, 0)
        far_share(g, 1)
        slot(1, last, range(splits[2], splits[3] + 1))
        far_share(g, 2)
        far_x(1)
        far_share(1 - g, 1)
        slot(1, last, range(splits[3] + 1, splits[3] + 2))
        far_x(2)
        far_share(1 - g, 2)

    def parts(b, act):
        @pl.when(lax.rem(b, n_fs) == far)
        def _():
            for i in range(3):
                if shares[i][1] > 0:
                    for j in range(1, n_tp):
                        act(part_copy(b, shares[i], i, j))

        @pl.when(lax.rem(b, n_fs) != far)
        def _():
            for j in range(1, n_tp):
                act(part_copy(b, whole_block, 0, j))

    loads = [
        pltpu.make_async_copy(up_hbm, stage.at[0], load_sem.at[0]),
        pltpu.make_async_copy(tok_hbm, tok_ref, load_sem.at[1]),
        pltpu.make_async_copy(down_hbm, stage.at[1], load_sem.at[2]),
    ]
    loads[0].start()
    loads[1].start()

    barrier = pltpu.get_barrier_semaphore()

    def greet(device):
        pl.semaphore_signal(barrier, inc=1, device_id=device, device_id_type=MESH)

    greet((1 - g, z, t))
    for j in range(1, n_tp):
        greet((g, z, lax.rem(t + j, n_tp)))
    pl.when(has_right)(lambda: greet((g, z + 1, t)))
    pl.when(has_left)(lambda: greet((g, z - 1, t)))

    def round_up(k):
        start, size = tables[0][k]
        row = pl.ds(pl.multiple_of((g * n_fs + z) * rows + start, 16), size)
        up_ref[row, :] = (stage[0, start : start + size] * gain[start : start + size]).astype(up_ref.dtype)

    def send_own(k):
        x_copy(0, z, k, g).start()
        if k < count(0):
            send_both(0, k)

    own = pl.ds(pl.multiple_of((g * n_fs + z) * rows, rows), rows)
    square = (rows, rows)
    on_diagonal = lax.broadcasted_iota(jnp.int32, square, 0) == lax.broadcasted_iota(jnp.int32, square, 1)
    gain = jnp.sum(jnp.where(on_diagonal, gain_ref[...], 0.0), axis=1, keepdims=True)
    loads[0].wait()
    order = [count(0)] + list(range(count(0)))
    round_up(order[0])
    round_up(order[1])
    pl.semaphore_wait(barrier, n_tp + has_right.astype(jnp.int32) + has_left.astype(jnp.int32))
    for i, k in enumerate(order):
        send_own(k)
        if i + 2 < len(order):
            round_up(order[i + 2])
    send_both(0, count(0))
    loads[2].start()

    loads[1].wait()
    floats = tok_ref[...].astype(jnp.float32)
    mean_square = jnp.mean(floats * floats, axis=1, keepdims=True)
    normed[pl.ds(pl.multiple_of(t * local, local), local), :] = (
        floats * lax.rsqrt(mean_square + 1e-06)
    ).astype(normed.dtype)
    for j in range(1, n_tp):
        token_copy(j).start()
    other_xz(0)
    loads[2].wait()
    down_ref[own, :] = stage[1].astype(down_ref.dtype)

    for s in range(1, last):
        slot(0, s)
    own_z(1)
    if last > 0:
        slot(0, last)
    own_x(1)

    for zz in range(n_fs):
        for k in range(count(0)):
            x_copy(0, zz, k, 1 - g).wait_recv()
    for j in range(1, n_tp):
        token_copy(j).wait_recv()

    tile = 256

    def first(i, carry):
        columns = pl.ds(pl.multiple_of(i * tile, tile), tile)
        pre = jnp.dot(normed[...], up_ref[:, columns], preferred_element_type=jnp.float32)
        hidden[:, columns] = jnp.square(jnp.maximum(pre, 0.0)).astype(hidden.dtype)
        return carry

    lax.fori_loop(0, width // tile, first, 0)

    other_xz(1)
    second(0)
    for s in range(1, last):
        slot(1, s)
        second(s)
    far_blocks()

    final = (1 - g) * n_fs + far
    last_tile = (final * rows + rows - 1) // 128

    def arrivals(b, carry):
        @pl.when(b != final)
        def _():
            parts(b, lambda copy: copy.wait_recv())

        return carry

    lax.fori_loop(0, n_gr * n_fs, arrivals, 0)
    for i in range(2):
        if shares[i][1] > 0:
            for j in range(1, n_tp):
                part_copy(final, shares[i], i, j).wait_recv()

    def total(i, carry):
        row = pl.ds(pl.multiple_of(i * 128, 128), 128)
        acc = part[row, pl.ds(pl.multiple_of(t * local, local), local)].astype(jnp.float32)
        for j in range(1, n_tp):
            acc = acc + arrived[j - 1, row, :].astype(jnp.float32)
        out_ref[:, row] = acc.T.astype(out_ref.dtype)
        return carry

    lax.fori_loop(0, last_tile, total, 0)
    lax.fori_loop(last_tile + 1, depth // 128, total, 0)

    def sent_parts(b, carry):
        parts(b, lambda copy: copy.wait_send())
        return carry

    lax.fori_loop(0, n_gr * n_fs, sent_parts, 0)
    for j in range(1, n_tp):
        token_copy(j).wait_send()

    def sent_blocks(zz, carry):
        for p in range(2):
            for k in range(count(p) + 2):
                pl.when(has_right & (zz <= z))(lambda: z_copy(p, zz, k, True).wait_send())
                pl.when(has_left & (zz >= z))(lambda: z_copy(p, zz, k, False).wait_send())
                if k < count(p):
                    x_copy(p, zz, k, g).wait_send()
                elif k == count(p):
                    pl.when(zz == z)(lambda: x_copy(p, zz, k, g).wait_send())
        return carry

    lax.fori_loop(0, n_fs, sent_blocks, 0)

    for j in range(1, n_tp):
        part_copy(final, shares[2], 2, j).wait_recv()
    total(last_tile, 0)


def solution(mesh):
    n_gr, n_fs, n_tp = (mesh.shape[a] for a in ("gr", "fs", "tp"))

    def on_device(prompt_tokens, norm_gain, up_master, down_master):
        local, depth = prompt_tokens.shape
        rows, width = up_master.shape
        blocks = n_gr * n_fs
        most = 2 + -(-rows // max(16, CHUNK_BYTES // (2 * width) // 16 * 16))
        dma = pltpu.SemaphoreType.DMA
        bf16 = jnp.bfloat16
        anywhere = pl.BlockSpec(memory_space=pl.ANY)
        vmem = pl.BlockSpec(memory_space=pltpu.VMEM)
        return pl.pallas_call(
            functools.partial(kernel, (n_gr, n_fs, n_tp)),
            out_shape=(
                pltpu.VMEM((depth, width), bf16),
                pltpu.VMEM((depth, width), bf16),
                jax.ShapeDtypeStruct((local, depth), bf16),
            ),
            in_specs=[anywhere, vmem, anywhere, anywhere],
            out_specs=(vmem, vmem, vmem),
            scratch_shapes=[
                pltpu.VMEM((local, depth), bf16),
                pltpu.VMEM((2, rows, width), jnp.float32),
                pltpu.VMEM((local * n_tp, depth), bf16),
                pltpu.VMEM((local * n_tp, width), bf16),
                pltpu.VMEM((depth, local * n_tp), bf16),
                pltpu.VMEM((n_tp - 1, depth, local), bf16),
                dma((3,)), dma((n_tp - 1,)), dma((n_tp - 1,)),
                dma((2, n_fs, most)), dma((2, n_fs, most)), dma((2, n_fs, most)),
                dma((2, n_fs, most)), dma((2, n_fs, most)),
                dma((blocks, 3, n_tp - 1)), dma((blocks, 3, n_tp - 1)),
            ],
            compiler_params=pltpu.CompilerParams(
                collective_id=0, has_side_effects=True, vmem_limit_bytes=44 * 2**20
            ),
        )(prompt_tokens, norm_gain[None, :], up_master, down_master)

    placed = (
        P(("gr", "fs", "tp"), None),
        P(("gr", "fs")),
        P(("gr", "fs"), "tp"),
        P(("gr", "fs"), "tp"),
    )
    return jax.shard_map(
        on_device,
        mesh=mesh,
        in_specs=placed,
        out_specs=(P(None, "tp"), P(None, "tp"), P(("gr", "fs", "tp"), None)),
        check_vma=False,
    )
```

profile of v0, /device:TPU:0, one launch (start us, length us, event | category | flops | bytes accessed | tf_op | source)
XLA Modules:
  0.0 183.0 jit_solution(15150659070226047703)
XLA Ops:
  0.6 174.8 %shard_map.67 = (bf16[2048,2048]{1,0:T(8,128)(2,1)S(1)}, bf16[2048,2048]{1,0:T(8,128)(2,1)S(1)}, bf16[128,2048]{1,0:T(8,128)(2,1)}) custom-call(bf16[128,2048]{1,0:T(8,128)(2,1)} %tok_hbm.1, f32[1,256]{1,0:T(1,128)} %bitcast.1, f32[256,2048]{1,0:T(8,128)} %up_hbm.1, f32[256,2048]{1,0:T(8,128)} %down_hbm.1), custom_call_target="tpu_custom_call" | custom-call | tf_op jit(solution)/shard_map/pallas_call | solution.py:354
  175.4 3.4 %copy.10 = bf16[2048,2048]{1,0:T(8,128)(2,1)} copy(bf16[2048,2048]{1,0:T(8,128)(2,1)S(1)} %get-tuple-element.3) | data formatting | bytes 16777216
  178.8 0.0 copy-start
  178.8 3.4 %copy.11 = bf16[2048,2048]{1,0:T(8,128)(2,1)} copy(bf16[2048,2048]{1,0:T(8,128)(2,1)S(1)} %get-tuple-element.4) | data formatting | bytes 16777216
  182.2 0.0 copy-done
  182.2 0.8 copy.12
Async XLA Ops:
  178.8 3.4 %copy-start = (bf16[128,2048]{1,0:T(8,128)(2,1)S(1)}, bf16[128,2048]{1,0:T(8,128)(2,1)}, u32[]{:S(2)}) copy-start(bf16[128,2048]{1,0:T(8,128)(2,1)} %get-tuple-element.11) | copy-start | bytes 1572868
where the time goes:
time: 183 us
  Pallas kernels  175 us (96%)
  local copies, waits for them, and re-layouts  7.59 us (4%)
    pallas_call x1, Pallas kernels, on_device(): pl.pallas_call(functools.partial(kernel, (n_gr, n_fs, n_tp)), out_shape=(...  175 us
    unnamed x5, local copies, waits for them, and re-layouts  7.59 us

commit v1 on v0

--- a/solution.py
+++ b/solution.py
@@ -9,6 +9,7 @@
 
 MESH = pl.DeviceIdType.MESH
 CHUNK_BYTES = 256 * 1024
+WRITES = 8
 
 
 def pieces_of(rows, most):
@@ -339,6 +340,20 @@
     total(last_tile, 0)
 
 
+def write_out(*refs):
+    held, outs, sem = refs[:3], refs[3:6], refs[6]
+    copies = []
+    for i, (src, dst) in enumerate(zip(held, outs)):
+        rows = src.shape[0] // WRITES
+        for k in range(WRITES):
+            part = pl.ds(k * rows, rows)
+            copies.append(pltpu.make_async_copy(src.at[part, :], dst.at[part, :], sem.at[i, k]))
+    for copy in copies:
+        copy.start()
+    for copy in copies:
+        copy.wait()
+
+
 def solution(mesh):
     n_gr, n_fs, n_tp = (mesh.shape[a] for a in ("gr", "fs", "tp"))
 
@@ -351,12 +366,12 @@
         bf16 = jnp.bfloat16
         anywhere = pl.BlockSpec(memory_space=pl.ANY)
         vmem = pl.BlockSpec(memory_space=pltpu.VMEM)
-        return pl.pallas_call(
+        held = pl.pallas_call(
             functools.partial(kernel, (n_gr, n_fs, n_tp)),
             out_shape=(
                 pltpu.VMEM((depth, width), bf16),
                 pltpu.VMEM((depth, width), bf16),
-                jax.ShapeDtypeStruct((local, depth), bf16),
+                pltpu.VMEM((local, depth), bf16),
             ),
             in_specs=[anywhere, vmem, anywhere, anywhere],
             out_specs=(vmem, vmem, vmem),
@@ -376,6 +391,18 @@
                 collective_id=0, has_side_effects=True, vmem_limit_bytes=44 * 2**20
             ),
         )(prompt_tokens, norm_gain[None, :], up_master, down_master)
+        return pl.pallas_call(
+            write_out,
+            out_shape=(
+                jax.ShapeDtypeStruct((depth, width), bf16),
+                jax.ShapeDtypeStruct((depth, width), bf16),
+                jax.ShapeDtypeStruct((local, depth), bf16),
+            ),
+            in_specs=[vmem, vmem, vmem],
+            out_specs=(anywhere, anywhere, anywhere),
+            scratch_shapes=[dma((3, WRITES))],
+            compiler_params=pltpu.CompilerParams(vmem_limit_bytes=2**20),
+        )(*held)
 
     placed = (
         P(("gr", "fs", "tp"), None),

time: 183 us -> 181 us (0.989)
  local copies, waits for them, and re-layouts: 7.59 us -> 0 us
  Pallas kernels: 175 us -> 180 us
    unnamed x5 -> x0, local copies, waits for them, and re-layouts: 7.59 us -> none
    pallas_call x0 -> x1, Pallas kernels: none -> 6.15 us  [on_device(): pl.pallas_call(write_out, out_shape=(jax.ShapeDtypeStruct((depth, width),...]
where the time goes in v1:
time: 181 us
  Pallas kernels  180 us (99%)
    pallas_call x1, Pallas kernels, on_device(): pl.pallas_call(functools.partial(kernel, (n_gr, n_fs, n_tp)), out_shape=(...  174 us
    pallas_call x1, Pallas kernels, on_device(): pl.pallas_call(write_out, out_shape=(jax.ShapeDtypeStruct((depth, width),...  6.15 us

profile of v1, /device:TPU:0, one launch (start us, length us, event | category | flops | bytes accessed | tf_op | source)
XLA Modules:
  0.0 180.8 jit_solution(3737410308074085799)
XLA Ops:
  0.6 174.0 %shard_map.67 = (bf16[2048,2048]{1,0:T(8,128)(2,1)S(1)}, bf16[2048,2048]{1,0:T(8,128)(2,1)S(1)}, bf16[128,2048]{1,0:T(8,128)(2,1)S(1)}) custom-call(bf16[128,2048]{1,0:T(8,128)(2,1)} %tok_hbm.1, f32[1,256]{1,0:T(1,128)} %bitcast.1, f32[256,2048]{1,0:T(8,128)} %up_hbm.1, f32[256,2048]{1,0:T(8,128)} %down_hbm.1), custom_call_target="tpu_custom_call" | custom-call | tf_op jit(solution)/shard_map/pallas_call | solution.py:369
  174.6 6.1 %shard_map.68 = (bf16[2048,2048]{1,0:T(8,128)(2,1)}, bf16[2048,2048]{1,0:T(8,128)(2,1)}, bf16[128,2048]{1,0:T(8,128)(2,1)}) custom-call(bf16[2048,2048]{1,0:T(8,128)(2,1)S(1)} %get-tuple-element.6.refs_0_, bf16[2048,2048]{1,0:T(8,128)(2,1)S(1)} %get-tuple-element.7.refs_1_, bf16[128,2048]{1,0:T(8,128)(2,1)S(1)} %get-tuple-element.8.refs_2_), custom_call_target="tpu_custom_call" | custom-call | tf_op jit(solution)/shard_map/pallas_call | solution.py:394

commit v2 on v1

v2 whole, which is shorter than its diff:
```python
import functools

import jax
import jax.numpy as jnp
from jax import lax
from jax.experimental import pallas as pl
from jax.experimental.pallas import tpu as pltpu
from jax.sharding import PartitionSpec as P

MESH = pl.DeviceIdType.MESH
CHUNK_BYTES = 256 * 1024
WRITES = 8
CROSSED = (3, 2)


def pieces_of(start, stop, most):
    rows = stop - start
    count = -(-rows // most)
    units = rows // 16
    cuts = [start + 16 * (units * i // count) for i in range(count)] + [stop]
    return [(a, b - a) for a, b in zip(cuts, cuts[1:])]


def split_rows(rows, width):
    most = max(16, CHUNK_BYTES // (2 * width) // 16 * 16)
    tail = max(0, rows - 128)
    tables = []
    for p in range(2):
        edge = rows - max(16, rows * CROSSED[p] // 256 * 16)
        cut = min(tail, edge) if p else edge
        near, rest, cross = pieces_of(0, cut, most), pieces_of(cut, edge, most), [(edge, rows - edge)]
        tables.append((near, rest, near + rest + cross + cross + rest))
    return tail, tables


def kernel(
    sizes, gain_hbm, tok_hbm, up_hbm, down_hbm,
    up_ref, down_ref, out_ref,
    tok_ref, gain_ref, stage, normed, hidden, part, arrived,
    far_hidden, far_part, far_arrived, far_out,
    load_sem, up_sem, tok_send, tok_recv,
    z_recv, right_send, left_send, x_recv, x_send, part_send, part_recv,
    hid_send, hid_recv, far_send, far_recv, give_send, give_recv,
):
    n_gr, n_fs, n_tp = sizes
    g, z, t = lax.axis_index("gr"), lax.axis_index("fs"), lax.axis_index("tp")
    rows, width = stage.shape[1:]
    local = tok_ref.shape[0]
    depth = up_ref.shape[0]
    last = n_fs - 1
    has_right, has_left = z < last, z > 0
    at_end = (z == 0) | (z == last)
    masters = (up_ref, down_ref)

    tail, tables = split_rows(rows, width)
    helped = n_fs >= 4 and rows % 128 == 0
    near = [range(len(a)) for a, _, _ in tables]
    rest = [range(len(a), len(a) + len(b)) for a, b, _ in tables]
    cross = [r.stop for r in rest]
    extra = [range(c + 2, c + 2 + len(r)) for c, r in zip(cross, rest)]

    def is_end(zz):
        return (zz == 0) | (zz == last)

    def rest_by_x(zz):
        return jnp.logical_not(is_end(zz)) | (zz == z) | (zz + z == last)

    def at(p, col, zz, k):
        start, size = tables[p][2][k]
        base = pl.multiple_of((col * n_fs + zz) * rows, rows)
        return masters[p].at[pl.ds(pl.multiple_of(base + start, 16), size), :]

    def z_copy(p, zz, k, right):
        ref = at(p, 1 - g if k > cross[p] else g, zz, k)
        send = right_send if right else left_send
        return pltpu.make_async_remote_copy(
            src_ref=ref, dst_ref=ref, send_sem=send.at[p, zz, k], recv_sem=z_recv.at[p, zz, k],
            device_id=(g, jnp.where(has_right, z + 1, z - 1) if right else jnp.where(has_left, z - 1, z + 1), t),
            device_id_type=MESH,
        )

    def x_copy(p, zz, k, col):
        ref = at(p, col, zz, k)
        return pltpu.make_async_remote_copy(
            src_ref=ref, dst_ref=ref, send_sem=x_send.at[p, zz, k], recv_sem=x_recv.at[p, zz, k],
            device_id=(1 - g, z, t), device_id_type=MESH,
        )

    def goes(p, zz, k, right):
        if k < cross[p] + 2:
            return has_right if right else has_left
        return (zz == 0) & (z + 1 < last) if right else (zz == last) & (z > 1)

    def send_both(p, k):
        pl.when(goes(p, z, k, True))(lambda: z_copy(p, z, k, True).start())
        pl.when(goes(p, z, k, False))(lambda: z_copy(p, z, k, False).start())

    def own_z(p):
        for k in range(cross[p] + 1):
            send_both(p, k)

    def own_x(p):
        for k in (cross[p], *rest[p], *near[p]):
            x_copy(p, z, k, g).start()

    def other_xz(p):
        x_copy(p, z, cross[p], 1 - g).wait_recv()
        send_both(p, cross[p] + 1)

    def other_rest(p):
        @pl.when(at_end)
        def _():
            for k, wide in zip(rest[p], extra[p]):
                x_copy(p, z, k, 1 - g).wait_recv()
                send_both(p, wide)

    def slot(p, s, items):
        for k in items:
            wide = k in extra[p]

            def come(right):
                zz = z - s if right else z + s
                z_copy(p, zz, k, right).wait_recv()
                if s < last:
                    pl.when(goes(p, zz, k, right))(lambda: z_copy(p, zz, k, right).start())
                if k in near[p]:
                    x_copy(p, zz, k, g).start()
                elif k in rest[p]:
                    pl.when(rest_by_x(zz))(lambda: x_copy(p, zz, k, g).start())

            from_left, from_right = z - s >= 0, z + s <= last
            if wide:
                from_left, from_right = (z - s == 0) & has_right, (z + s == last) & has_left
            if not wide or s < last:
                pl.when(from_left)(lambda: come(True))
                pl.when(from_right)(lambda: come(False))

    def whole_slot(p, s):
        slot(p, s, range(len(tables[p][2])))

    def token_copy(j):
        mine = normed.at[pl.ds(pl.multiple_of(t * local, local), local), :]
        return pltpu.make_async_remote_copy(
            src_ref=mine, dst_ref=mine, send_sem=tok_send.at[j - 1], recv_sem=tok_recv.at[j - 1],
            device_id=(g, z, lax.rem(t + j, n_tp)), device_id_type=MESH,
        )

    far = jnp.where(z + z >= last, 0, last)
    shares = [(0, tail), (tail, rows - tail)]
    whole_block = (0, rows)

    def part_copy(block, share, i, j):
        to = lax.rem(t + j, n_tp)
        start, size = share
        base = pl.multiple_of(block * rows, rows)
        row = pl.ds(pl.multiple_of(base + start, 16), size)
        return pltpu.make_async_remote_copy(
            src_ref=part.at[row, pl.ds(pl.multiple_of(to * local, local), local)],
            dst_ref=arrived.at[j - 1, row, :],
            send_sem=part_send.at[block, i, j - 1], recv_sem=part_recv.at[block, i, j - 1],
            device_id=(g, z, to), device_id_type=MESH,
        )

    def product(block, share, values):
        start, size = share
        base = pl.multiple_of(block * rows, rows)
        row = pl.ds(pl.multiple_of(base + start, 16), size)
        return row, lax.dot_general(
            down_ref[row, :], values[...], (((1,), (1,)), ((), ())),
            preferred_element_type=jnp.float32,
        ).astype(part.dtype)

    def multiply(block, share, i):
        row, value = product(block, share, hidden)
        part[row, :] = value
        for j in range(1, n_tp):
            part_copy(block, share, i, j).start()

    def second(s):
        def one(i, carry):
            other, side = i // 2, lax.rem(i, 2)
            dist = s - other
            zz = z + (2 * side - 1) * dist
            ok = (dist >= 0) & (zz >= 0) & (zz <= last) & ((dist > 0) | (side == 0)) & (zz != far)

            @pl.when(ok)
            def _():
                @pl.when(other == 1)
                def _():
                    for k in near[1]:
                        x_copy(1, zz, k, 1 - g).wait_recv()

                    @pl.when(jnp.logical_not(is_end(zz)))
                    def _():
                        for k in rest[1]:
                            x_copy(1, zz, k, 1 - g).wait_recv()

                multiply(jnp.where(other == 1, 1 - g, g) * n_fs + zz, whole_block, 0)

            return carry

        lax.fori_loop(0, 4, one, 0)

    def far_share(col, i):
        if shares[i][1] > 0:
            multiply(col * n_fs + far, shares[i], i)

    def far_tails():
        far_share(g, 1)
        far_share(1 - g, 1)

    tail_here = jnp.logical_not(at_end) if helped else z >= 0
    helping = (z == 1) | (z == last - 1)
    helper = jnp.where(z == 0, 1, last - 1)
    ward = jnp.where(z == 1, 0, last)

    def hidden_copy(i):
        row = pl.ds(i * local, local)
        return pltpu.make_async_remote_copy(
            src_ref=hidden.at[row, :], dst_ref=far_hidden.at[row, :],
            send_sem=hid_send.at[i], recv_sem=hid_recv.at[i],
            device_id=(g, helper, t), device_id_type=MESH,
        )

    def far_copy(col, j):
        to = lax.rem(t + j, n_tp)
        row = pl.ds(col * 128, 128)
        return pltpu.make_async_remote_copy(
            src_ref=far_part.at[row, pl.ds(pl.multiple_of(to * local, local), local)],
            dst_ref=far_arrived.at[j - 1, row, :],
            send_sem=far_send.at[col, j - 1], recv_sem=far_recv.at[col, j - 1],
            device_id=(g, z, to), device_id_type=MESH,
        )

    def give_copy(col):
        column = pl.ds(pl.multiple_of((col * n_fs + far) * rows + tail, 128), 128)
        return pltpu.make_async_remote_copy(
            src_ref=far_out.at[col], dst_ref=out_ref.at[:, column],
            send_sem=give_send.at[col], recv_sem=give_recv.at[col],
            device_id=(g, ward, t), device_id_type=MESH,
        )

    def help_multiply():
        for i in range(n_tp):
            hidden_copy(i).wait_recv()
        for col in range(2):
            _, value = product(col * n_fs + far, shares[1], far_hidden)
            far_part[pl.ds(col * 128, 128), :] = value
            for j in range(1, n_tp):
                far_copy(col, j).start()

    def help_total():
        for col in range(2):
            for j in range(1, n_tp):
                far_copy(col, j).wait_recv()
            row = pl.ds(col * 128, 128)
            acc = far_part[row, pl.ds(pl.multiple_of(t * local, local), local)].astype(jnp.float32)
            for j in range(1, n_tp):
                acc = acc + far_arrived[j - 1, row, :].astype(jnp.float32)
            far_out[col] = acc.T.astype(far_out.dtype)
            give_copy(col).start()

    def parts(b, act, final_too=True):
        @pl.when(lax.rem(b, n_fs) == far)
        def _():
            if shares[0][1] > 0:
                for j in range(1, n_tp):
                    if final_too:
                        act(part_copy(b, shares[0], 0, j))
                    else:
                        pl.when(b != final)(lambda: act(part_copy(b, shares[0], 0, j)))

            @pl.when(tail_here)
            def _():
                for j in range(1, n_tp):
                    act(part_copy(b, shares[1], 1, j))

        @pl.when(lax.rem(b, n_fs) != far)
        def _():
            for j in range(1, n_tp):
                act(part_copy(b, whole_block, 0, j))

    barrier = pltpu.get_barrier_semaphore()

    def greet(device):
        pl.semaphore_signal(barrier, inc=1, device_id=device, device_id_type=MESH)

    greet((1 - g, z, t))
    pl.when(has_right)(lambda: greet((g, z + 1, t)))
    pl.when(has_left)(lambda: greet((g, z - 1, t)))
    for j in range(1, n_tp):
        greet((g, z, lax.rem(t + j, n_tp)))

    order = [cross[0], *near[0]]

    def up_load(k):
        start, size = tables[0][2][k]
        row = pl.ds(start, size)
        return pltpu.make_async_copy(up_hbm.at[row, :], stage.at[0, row, :], up_sem.at[k])

    loads = [
        pltpu.make_async_copy(gain_hbm, gain_ref, load_sem.at[0]),
        pltpu.make_async_copy(tok_hbm, tok_ref, load_sem.at[1]),
        pltpu.make_async_copy(down_hbm, stage.at[1], load_sem.at[2]),
    ]
    loads[0].start()
    for k in order:
        up_load(k).start()
    loads[1].start()
    loads[2].start()

    def round_up(k):
        start, size = tables[0][2][k]
        row = pl.ds(pl.multiple_of((g * n_fs + z) * rows + start, 16), size)
        up_load(k).wait()
        up_ref[row, :] = (stage[0, start : start + size] * gain[start : start + size]).astype(up_ref.dtype)

    def send_own(k):
        x_copy(0, z, k, g).start()
        if k != cross[0]:
            send_both(0, k)

    own = pl.ds(pl.multiple_of((g * n_fs + z) * rows, rows), rows)
    square = (rows, rows)
    on_diagonal = lax.broadcasted_iota(jnp.int32, square, 0) == lax.broadcasted_iota(jnp.int32, square, 1)
    loads[0].wait()
    gain = jnp.sum(jnp.where(on_diagonal, gain_ref[...], 0.0), axis=1, keepdims=True)
    round_up(order[0])
    round_up(order[1])
    pl.semaphore_wait(barrier, n_tp + has_right.astype(jnp.int32) + has_left.astype(jnp.int32))
    for i, k in enumerate(order):
        send_own(k)
        if i + 2 < len(order):
            round_up(order[i + 2])
    send_both(0, cross[0])

    loads[1].wait()
    floats = tok_ref[...].astype(jnp.float32)
    mean_square = jnp.mean(floats * floats, axis=1, keepdims=True)
    normed[pl.ds(pl.multiple_of(t * local, local), local), :] = (
        floats * lax.rsqrt(mean_square + 1e-06)
    ).astype(normed.dtype)
    for j in range(1, n_tp):
        token_copy(j).start()
    other_xz(0)
    loads[2].wait()
    down_ref[own, :] = stage[1].astype(down_ref.dtype)

    for s in range(1, last):
        whole_slot(0, s)
    own_z(1)
    if last > 0:
        slot(0, last, near[0])
    own_x(1)
    if last > 0:
        slot(0, last, range(cross[0], cross[0] + 2))

    for zz in range(n_fs):
        for k in near[0]:
            x_copy(0, zz, k, 1 - g).wait_recv()
    for j in range(1, n_tp):
        token_copy(j).wait_recv()

    tile = 256

    def first(i, carry):
        columns = pl.ds(pl.multiple_of(i * tile, tile), tile)
        pre = jnp.dot(normed[...], up_ref[:, columns], preferred_element_type=jnp.float32)
        hidden[:, columns] = jnp.square(jnp.maximum(pre, 0.0)).astype(hidden.dtype)
        return carry

    lax.fori_loop(0, width // tile, first, 0)

    other_xz(1)
    other_rest(1)
    if helped:
        @pl.when(at_end)
        def _():
            for i in range(n_tp):
                hidden_copy(i).start()

    second(0)
    for s in range(1, last):
        whole_slot(1, s)
        second(s)
    slot(1, last, near[1])
    second(last)
    far_share(g, 0)
    slot(1, last, rest[1])
    if helped:
        pl.when(tail_here)(far_tails)
        pl.when(helping)(help_multiply)
    for k in near[1]:
        x_copy(1, far, k, 1 - g).wait_recv()
    far_share(1 - g, 0)
    if helped:
        pl.when(helping)(help_total)

    def last_in():
        slot(1, last, range(cross[1], cross[1] + 2))

        @pl.when(at_end)
        def _():
            for k in rest[1]:
                x_copy(1, far, k, 1 - g).wait_recv()

    if not helped:
        last_in()
        far_tails()

    final = (1 - g) * n_fs + far
    final_tile = final * (rows // 128)
    last_tile = final_tile + tail // 128

    def arrivals(b, carry):
        parts(b, lambda copy: copy.wait_recv(), False)
        return carry

    lax.fori_loop(0, n_gr * n_fs, arrivals, 0)

    def total(i, carry):
        row = pl.ds(pl.multiple_of(i * 128, 128), 128)
        acc = part[row, pl.ds(pl.multiple_of(t * local, local), local)].astype(jnp.float32)
        for j in range(1, n_tp):
            acc = acc + arrived[j - 1, row, :].astype(jnp.float32)
        out_ref[:, row] = acc.T.astype(out_ref.dtype)
        return carry

    def total_if(i, carry):
        is_tail = (lax.rem(i * 128, rows) == tail) & (lax.rem(i * 128 // rows, n_fs) == far)

        @pl.when(tail_here | jnp.logical_not(is_tail))
        def _():
            total(i, 0)

        return carry

    lax.fori_loop(0, final_tile, total_if, 0)
    lax.fori_loop(last_tile, depth // 128, total_if, 0)

    def sent_parts(b, carry):
        parts(b, lambda copy: copy.wait_send())
        return carry

    if shares[0][1] > 0:
        for j in range(1, n_tp):
            part_copy(final, shares[0], 0, j).wait_recv()
    lax.fori_loop(final_tile, last_tile, total, 0)
    lax.fori_loop(0, n_gr * n_fs, sent_parts, 0)
    for j in range(1, n_tp):
        token_copy(j).wait_send()
    if helped:
        @pl.when(at_end)
        def _():
            for i in range(n_tp):
                hidden_copy(i).wait_send()

        @pl.when(helping)
        def _():
            for col in range(2):
                for j in range(1, n_tp):
                    far_copy(col, j).wait_send()

    def sent_blocks(zz, carry):
        for p in range(2):
            for k in range(len(tables[p][2])):
                pl.when(goes(p, zz, k, True) & (zz <= z))(lambda: z_copy(p, zz, k, True).wait_send())
                pl.when(goes(p, zz, k, False) & (zz >= z))(lambda: z_copy(p, zz, k, False).wait_send())
                if k in near[p]:
                    x_copy(p, zz, k, g).wait_send()
                elif k in rest[p]:
                    pl.when(rest_by_x(zz))(lambda: x_copy(p, zz, k, g).wait_send())
                elif k == cross[p]:
                    pl.when(zz == z)(lambda: x_copy(p, zz, k, g).wait_send())
        return carry

    lax.fori_loop(0, n_fs, sent_blocks, 0)
    if helped:
        last_in()

        @pl.when(at_end)
        def _():
            for col in range(2):
                give_copy(col).wait_recv()

        @pl.when(helping)
        def _():
            for col in range(2):
                give_copy(col).wait_send()


def write_out(*refs):
    held, outs, sem = refs[:3], refs[3:6], refs[6]
    copies = []
    for i, (src, dst) in enumerate(zip(held, outs)):
        rows = src.shape[0] // WRITES
        for k in range(WRITES):
            part = pl.ds(k * rows, rows)
            copies.append(pltpu.make_async_copy(src.at[part, :], dst.at[part, :], sem.at[i, k]))
    for copy in copies:
        copy.start()
    for copy in copies:
        copy.wait()


def solution(mesh):
    n_gr, n_fs, n_tp = (mesh.shape[a] for a in ("gr", "fs", "tp"))

    def on_device(prompt_tokens, norm_gain, up_master, down_master):
        local, depth = prompt_tokens.shape
        rows, width = up_master.shape
        blocks = n_gr * n_fs
        most = max(len(table) for _, _, table in split_rows(rows, width)[1])
        dma = pltpu.SemaphoreType.DMA
        bf16 = jnp.bfloat16
        anywhere = pl.BlockSpec(memory_space=pl.ANY)
        vmem = pl.BlockSpec(memory_space=pltpu.VMEM)
        held = pl.pallas_call(
            functools.partial(kernel, (n_gr, n_fs, n_tp)),
            out_shape=(
                pltpu.VMEM((depth, width), bf16),
                pltpu.VMEM((depth, width), bf16),
                pltpu.VMEM((local, depth), bf16),
            ),
            in_specs=[anywhere] * 4,
            out_specs=(vmem, vmem, vmem),
            scratch_shapes=[
                pltpu.VMEM((local, depth), bf16),
                pltpu.VMEM((1, rows), jnp.float32),
                pltpu.VMEM((2, rows, width), jnp.float32),
                pltpu.VMEM((local * n_tp, depth), bf16),
                pltpu.VMEM((local * n_tp, width), bf16),
                pltpu.VMEM((depth, local * n_tp), bf16),
                pltpu.VMEM((n_tp - 1, depth, local), bf16),
                pltpu.VMEM((local * n_tp, width), bf16),
                pltpu.VMEM((256, local * n_tp), bf16),
                pltpu.VMEM((n_tp - 1, 256, local), bf16),
                pltpu.VMEM((2, local, 128), bf16),
                dma((3,)), dma((most,)), dma((n_tp - 1,)), dma((n_tp - 1,)),
                dma((2, n_fs, most)), dma((2, n_fs, most)), dma((2, n_fs, most)),
                dma((2, n_fs, most)), dma((2, n_fs, most)),
                dma((blocks, 2, n_tp - 1)), dma((blocks, 2, n_tp - 1)),
                dma((n_tp,)), dma((n_tp,)),
                dma((2, n_tp - 1)), dma((2, n_tp - 1)), dma((2,)), dma((2,)),
            ],
            compiler_params=pltpu.CompilerParams(
                collective_id=0, has_side_effects=True, vmem_limit_bytes=44 * 2**20
            ),
        )(norm_gain[None, :], prompt_tokens, up_master, down_master)
        return pl.pallas_call(
            write_out,
            out_shape=(
                jax.ShapeDtypeStruct((depth, width), bf16),
                jax.ShapeDtypeStruct((depth, width), bf16),
                jax.ShapeDtypeStruct((local, depth), bf16),
            ),
            in_specs=[vmem, vmem, vmem],
            out_specs=(anywhere, anywhere, anywhere),
            scratch_shapes=[dma((3, WRITES))],
            compiler_params=pltpu.CompilerParams(vmem_limit_bytes=2**20),
        )(*held)

    placed = (
        P(("gr", "fs", "tp"), None),
        P(("gr", "fs")),
        P(("gr", "fs"), "tp"),
        P(("gr", "fs"), "tp"),
    )
    return jax.shard_map(
        on_device,
        mesh=mesh,
        in_specs=placed,
        out_specs=(P(None, "tp"), P(None, "tp"), P(("gr", "fs", "tp"), None)),
        check_vma=False,
    )
```

time: 181 us -> 177 us (0.978)
  Pallas kernels: 180 us -> 176 us
    pallas_call x1, Pallas kernels: 174 us -> 170 us  [on_device(): pl.pallas_call(functools.partial(kernel, (n_gr, n_fs, n_tp)), out_shape=(...]
where the time goes in v2:
time: 177 us
  Pallas kernels  176 us (99%)
    pallas_call x1, Pallas kernels, on_device(): pl.pallas_call(functools.partial(kernel, (n_gr, n_fs, n_tp)), out_shape=(...  170 us
    pallas_call x1, Pallas kernels, on_device(): pl.pallas_call(write_out, out_shape=(jax.ShapeDtypeStruct((depth, width),...  6.15 us

profile of v2, /device:TPU:0, one launch (start us, length us, event | category | flops | bytes accessed | tf_op | source)
XLA Modules:
  0.0 177.1 jit_solution(13743412442617654466)
XLA Ops:
  0.6 170.3 %shard_map.67 = (bf16[2048,2048]{1,0:T(8,128)(2,1)S(1)}, bf16[2048,2048]{1,0:T(8,128)(2,1)S(1)}, bf16[128,2048]{1,0:T(8,128)(2,1)S(1)}) custom-call(f32[1,256]{1,0:T(1,128)} %bitcast.1, bf16[128,2048]{1,0:T(8,128)(2,1)} %tok_hbm.1, f32[256,2048]{1,0:T(8,128)} %up_hbm.1, f32[256,2048]{1,0:T(8,128)} %down_hbm.1), custom_call_target="tpu_custom_call" | custom-call | tf_op jit(solution)/shard_map/pallas_call | solution.py:518
  170.9 6.1 %shard_map.68 = (bf16[2048,2048]{1,0:T(8,128)(2,1)}, bf16[2048,2048]{1,0:T(8,128)(2,1)}, bf16[128,2048]{1,0:T(8,128)(2,1)}) custom-call(bf16[2048,2048]{1,0:T(8,128)(2,1)S(1)} %get-tuple-element.6.refs_0_, bf16[2048,2048]{1,0:T(8,128)(2,1)S(1)} %get-tuple-element.7.refs_1_, bf16[128,2048]{1,0:T(8,128)(2,1)S(1)} %get-tuple-element.8.refs_2_), custom_call_target="tpu_custom_call" | custom-call | tf_op jit(solution)/shard_map/pallas_call | solution.py:550

commit v3 on v2

v3 whole, which is shorter than its diff:
```python
import functools

import jax
import jax.numpy as jnp
from jax import lax
from jax.experimental import pallas as pl
from jax.experimental.pallas import tpu as pltpu
from jax.sharding import PartitionSpec as P

MESH = pl.DeviceIdType.MESH
PIECES = (3, 2, 1)
WRITES = 4


def pieces_of(start, stop, count):
    units = (stop - start) // 8
    cuts = [start + 8 * (units * i // count) for i in range(count)] + [stop]
    return [(a, b - a) for a, b in zip(cuts, cuts[1:]) if b > a]


def split_rows(rows):
    tail = max(0, rows - 128)
    edge = rows - max(8, rows * 5 // 256 * 8)
    tables = []
    for cut, pieces in ((edge, PIECES[0]), (min(tail, edge), PIECES[1])):
        near, rest, cross = pieces_of(0, cut, pieces), pieces_of(cut, edge, PIECES[2]), [(edge, rows - edge)]
        tables.append((near, rest, near + rest + cross + cross + rest))
    return tail, tables


def kernel(
    sizes, gain_hbm, tok_hbm, up_hbm, down_hbm,
    up_ref, down_ref, out_ref,
    tok_ref, gain_ref, stage, normed, hidden, part, arrived,
    far_hidden, far_part, far_arrived, far_out,
    load_sem, up_sem, tok_sem,
    z_recv, right_send, left_send, x_recv, x_send, part_send, part_recv,
    hid_sem, far_sem, give_sem,
):
    n_gr, n_fs, n_tp = sizes
    g, z, t = lax.axis_index("gr"), lax.axis_index("fs"), lax.axis_index("tp")
    rows, width = stage.shape[1:]
    local = tok_ref.shape[0]
    depth = up_ref.shape[0]
    last = n_fs - 1
    has_right, has_left = z < last, z > 0
    at_end = (z == 0) | (z == last)
    masters = (up_ref, down_ref)

    tail, tables = split_rows(rows)
    helped = n_fs >= 4 and rows % 128 == 0
    near = [range(len(a)) for a, _, _ in tables]
    rest = [range(len(a), len(a) + len(b)) for a, b, _ in tables]
    cross = [r.stop for r in rest]
    extra = [range(c + 2, c + 2 + len(r)) for c, r in zip(cross, rest)]

    def inner(zz):
        return (zz != 0) & (zz != last)

    def rest_by_x(zz, here):
        return inner(zz) | (zz == here) | (zz + here == last)

    def goes(p, zz, k, right, here):
        if k < cross[p] + 2:
            return here < last if right else here > 0
        return (zz == 0) & (here + 1 < last) if right else (zz == last) & (here > 1)

    def settled(ref, sem):
        pltpu.make_async_copy(ref, ref, sem).wait()

    def settled_rows(count, sem):
        if count:
            settled(up_ref.at[pl.ds(0, count), :], sem)

    def size_of(p, items):
        return sum(tables[p][2][k][1] for k in items)

    def at(p, col, zz, k):
        start, size = tables[p][2][k]
        base = pl.multiple_of((col * n_fs + zz) * rows, rows)
        return masters[p].at[pl.ds(pl.multiple_of(base + start, 8), size), :]

    def z_copy(p, zz, k, right):
        ref = at(p, 1 - g if k > cross[p] else g, zz, k)
        send = right_send if right else left_send
        return pltpu.make_async_remote_copy(
            src_ref=ref, dst_ref=ref, send_sem=send.at[p], recv_sem=z_recv.at[p, zz if right else zz - 1, k],
            device_id=(g, jnp.where(has_right, z + 1, z - 1) if right else jnp.where(has_left, z - 1, z + 1), t),
            device_id_type=MESH,
        )

    def x_sem(p, zz, k):
        if k == cross[p]:
            return x_recv.at[p]
        if p == 0:
            return x_recv.at[2]
        return x_recv.at[3 + zz + (0 if k in near[1] else n_fs)]

    def x_copy(p, zz, k, col):
        ref = at(p, col, zz, k)
        return pltpu.make_async_remote_copy(
            src_ref=ref, dst_ref=ref, send_sem=x_send.at[p], recv_sem=x_sem(p, zz, k),
            device_id=(1 - g, z, t), device_id_type=MESH,
        )

    def send_both(p, k):
        pl.when(goes(p, z, k, True, z))(lambda: z_copy(p, z, k, True).start())
        pl.when(goes(p, z, k, False, z))(lambda: z_copy(p, z, k, False).start())

    def own_z(p):
        for k in range(cross[p] + 1):
            send_both(p, k)

    def own_x(p):
        for k in (cross[p], *rest[p], *near[p]):
            x_copy(p, z, k, g).start()

    def other_xz(p):
        x_copy(p, z, cross[p], 1 - g).wait_recv()
        send_both(p, cross[p] + 1)

    def near_in(zz):
        settled_rows(size_of(1, near[1]), x_recv.at[3 + zz])

    def rest_in(zz):
        settled_rows(size_of(1, rest[1]), x_recv.at[3 + n_fs + zz])

    def other_rest(p):
        @pl.when(at_end)
        def _():
            rest_in(z)
            for wide in extra[p]:
                send_both(p, wide)

    def slot(p, s, items):
        for k in items:
            wide = k in extra[p]

            def come(right):
                zz = z - s if right else z + s
                z_copy(p, zz, k, right).wait_recv()
                if s < last:
                    pl.when(goes(p, zz, k, right, z))(lambda: z_copy(p, zz, k, right).start())
                if k in near[p]:
                    x_copy(p, zz, k, g).start()
                elif k in rest[p]:
                    pl.when(rest_by_x(zz, z))(lambda: x_copy(p, zz, k, g).start())

            from_left, from_right = z - s >= 0, z + s <= last
            if wide:
                from_left, from_right = (z - s == 0) & has_right, (z + s == last) & has_left
            if not wide or s < last:
                pl.when(from_left)(lambda: come(True))
                pl.when(from_right)(lambda: come(False))

    def whole_slot(p, s):
        slot(p, s, range(len(tables[p][2])))

    def token_copy(j):
        mine = normed.at[pl.ds(pl.multiple_of(t * local, local), local), :]
        return pltpu.make_async_remote_copy(
            src_ref=mine, dst_ref=mine, send_sem=tok_sem.at[0], recv_sem=tok_sem.at[1],
            device_id=(g, z, lax.rem(t + j, n_tp)), device_id_type=MESH,
        )

    far = jnp.where(z + z >= last, 0, last)
    shares = [(0, tail), (tail, rows - tail)]
    whole_block = (0, rows)

    def part_copy(block, share, j, final):
        to = lax.rem(t + j, n_tp)
        start, size = share
        base = pl.multiple_of(block * rows, rows)
        row = pl.ds(pl.multiple_of(base + start, 16), size)
        return pltpu.make_async_remote_copy(
            src_ref=part.at[row, pl.ds(pl.multiple_of(to * local, local), local)],
            dst_ref=arrived.at[j - 1, row, :],
            send_sem=part_send.at[0], recv_sem=part_recv.at[1 if final else 0],
            device_id=(g, z, to), device_id_type=MESH,
        )

    def product(block, share, values):
        start, size = share
        base = pl.multiple_of(block * rows, rows)
        row = pl.ds(pl.multiple_of(base + start, 16), size)
        return row, lax.dot_general(
            down_ref[row, :], values[...], (((1,), (1,)), ((), ())),
            preferred_element_type=jnp.float32,
        ).astype(part.dtype)

    def multiply(block, share, final=False):
        row, value = product(block, share, hidden)
        part[row, :] = value
        for j in range(1, n_tp):
            part_copy(block, share, j, final).start()

    def second(s):
        def one(i, carry):
            other, side = i // 2, lax.rem(i, 2)
            dist = s - other
            zz = z + (2 * side - 1) * dist
            ok = (dist >= 0) & (zz >= 0) & (zz <= last) & ((dist > 0) | (side == 0)) & (zz != far)

            @pl.when(ok)
            def _():
                @pl.when(other == 1)
                def _():
                    near_in(zz)
                    pl.when(inner(zz))(lambda: rest_in(zz))

                multiply(jnp.where(other == 1, 1 - g, g) * n_fs + zz, whole_block)

            return carry

        lax.fori_loop(0, 4, one, 0)

    def far_share(col, i, final=False):
        if shares[i][1] > 0:
            multiply(col * n_fs + far, shares[i], final)

    def far_tails():
        far_share(g, 1)
        far_share(1 - g, 1)

    tail_here = jnp.logical_not(at_end) if helped else z >= 0
    helping = (z == 1) | (z == last - 1)
    helper = jnp.where(z == 0, 1, last - 1)
    ward = jnp.where(z == 1, 0, last)

    def hidden_copy():
        return pltpu.make_async_remote_copy(
            src_ref=hidden, dst_ref=far_hidden, send_sem=hid_sem.at[0], recv_sem=hid_sem.at[1],
            device_id=(g, helper, t), device_id_type=MESH,
        )

    def far_copy(col, j):
        to = lax.rem(t + j, n_tp)
        row = pl.ds(col * 128, 128)
        return pltpu.make_async_remote_copy(
            src_ref=far_part.at[row, pl.ds(pl.multiple_of(to * local, local), local)],
            dst_ref=far_arrived.at[j - 1, row, :],
            send_sem=far_sem.at[0], recv_sem=far_sem.at[1],
            device_id=(g, z, to), device_id_type=MESH,
        )

    def give_copy(col):
        column = pl.ds(pl.multiple_of((col * n_fs + far) * rows + tail, 128), 128)
        return pltpu.make_async_remote_copy(
            src_ref=far_out.at[col], dst_ref=out_ref.at[:, column],
            send_sem=give_sem.at[0], recv_sem=give_sem.at[1],
            device_id=(g, ward, t), device_id_type=MESH,
        )

    def help_multiply():
        hidden_copy().wait_recv()
        for col in range(2):
            _, value = product(col * n_fs + far, shares[1], far_hidden)
            far_part[pl.ds(col * 128, 128), :] = value
            for j in range(1, n_tp):
                far_copy(col, j).start()

    def help_total():
        settled(far_arrived, far_sem.at[1])
        for col in range(2):
            row = pl.ds(col * 128, 128)
            acc = far_part[row, pl.ds(pl.multiple_of(t * local, local), local)].astype(jnp.float32)
            for j in range(1, n_tp):
                acc = acc + far_arrived[j - 1, row, :].astype(jnp.float32)
            far_out[col] = acc.T.astype(far_out.dtype)
            give_copy(col).start()

    def parts_settled(final_rows, sem):
        every = depth - final_rows
        if not helped:
            settled(arrived.at[:, pl.ds(0, every), :], sem)
            return
        pl.when(at_end)(lambda: settled(arrived.at[:, pl.ds(0, every - 256), :], sem))
        pl.when(tail_here)(lambda: settled(arrived.at[:, pl.ds(0, every), :], sem))

    barrier = pltpu.get_barrier_semaphore()

    def greet(device):
        pl.semaphore_signal(barrier, inc=1, device_id=device, device_id_type=MESH)

    greet((1 - g, z, t))
    pl.when(has_right)(lambda: greet((g, z + 1, t)))
    pl.when(has_left)(lambda: greet((g, z - 1, t)))
    for j in range(1, n_tp):
        greet((g, z, lax.rem(t + j, n_tp)))

    order = [cross[0], *near[0]]

    def up_load(k):
        start, size = tables[0][2][k]
        row = pl.ds(start, size)
        return pltpu.make_async_copy(up_hbm.at[row, :], stage.at[0, row, :], up_sem.at[k])

    loads = [
        pltpu.make_async_copy(gain_hbm, gain_ref, load_sem.at[0]),
        pltpu.make_async_copy(tok_hbm, tok_ref, load_sem.at[1]),
        pltpu.make_async_copy(down_hbm, stage.at[1], load_sem.at[2]),
    ]
    loads[0].start()
    for k in order:
        up_load(k).start()
    loads[1].start()
    loads[2].start()

    def round_up(k):
        start, size = tables[0][2][k]
        row = pl.ds(pl.multiple_of((g * n_fs + z) * rows + start, 8), size)
        up_load(k).wait()
        up_ref[row, :] = (stage[0, start : start + size] * gain[start : start + size]).astype(up_ref.dtype)

    def send_own(k):
        x_copy(0, z, k, g).start()
        if k != cross[0]:
            send_both(0, k)

    own = pl.ds(pl.multiple_of((g * n_fs + z) * rows, rows), rows)
    square = (rows, rows)
    on_diagonal = lax.broadcasted_iota(jnp.int32, square, 0) == lax.broadcasted_iota(jnp.int32, square, 1)
    loads[0].wait()
    gain = jnp.sum(jnp.where(on_diagonal, gain_ref[...], 0.0), axis=1, keepdims=True)
    round_up(order[0])
    round_up(order[1])
    pl.semaphore_wait(barrier, n_tp + has_right.astype(jnp.int32) + has_left.astype(jnp.int32))
    for i, k in enumerate(order):
        send_own(k)
        if i + 2 < len(order):
            round_up(order[i + 2])
    send_both(0, cross[0])

    loads[1].wait()
    floats = tok_ref[...].astype(jnp.float32)
    mean_square = jnp.mean(floats * floats, axis=1, keepdims=True)
    normed[pl.ds(pl.multiple_of(t * local, local), local), :] = (
        floats * lax.rsqrt(mean_square + 1e-06)
    ).astype(normed.dtype)
    for j in range(1, n_tp):
        token_copy(j).start()
    other_xz(0)
    loads[2].wait()
    down_ref[own, :] = stage[1].astype(down_ref.dtype)

    for s in range(1, last):
        whole_slot(0, s)
    own_z(1)
    if last > 0:
        slot(0, last, near[0])
    own_x(1)
    if last > 0:
        slot(0, last, range(cross[0], cross[0] + 2))

    settled_rows(n_fs * size_of(0, near[0]), x_recv.at[2])
    others = normed.at[pl.ds(0, (n_tp - 1) * local), :]
    settled(others, tok_sem.at[1])

    tile = 256

    def first(i, carry):
        columns = pl.ds(pl.multiple_of(i * tile, tile), tile)
        pre = jnp.dot(normed[...], up_ref[:, columns], preferred_element_type=jnp.float32)
        hidden[:, columns] = jnp.square(jnp.maximum(pre, 0.0)).astype(hidden.dtype)
        return carry

    lax.fori_loop(0, width // tile, first, 0)

    other_xz(1)
    other_rest(1)
    if helped:
        @pl.when(at_end)
        def _():
            hidden_copy().start()

    second(0)
    for s in range(1, last):
        whole_slot(1, s)
        second(s)
    slot(1, last, near[1])
    second(last)
    far_share(g, 0)
    slot(1, last, rest[1])
    if helped:
        pl.when(tail_here)(far_tails)
        pl.when(helping)(help_multiply)
    near_in(far)
    far_share(1 - g, 0, True)
    if helped:
        pl.when(helping)(help_total)

    def last_in():
        slot(1, last, range(cross[1], cross[1] + 2))

        pl.when(at_end)(lambda: rest_in(far))

    if not helped:
        last_in()
        far_tails()

    final = (1 - g) * n_fs + far
    final_tile = final * (rows // 128)
    last_tile = final_tile + tail // 128

    parts_settled(tail, part_recv.at[0])

    def total(i, carry):
        row = pl.ds(pl.multiple_of(i * 128, 128), 128)
        acc = part[row, pl.ds(pl.multiple_of(t * local, local), local)].astype(jnp.float32)
        for j in range(1, n_tp):
            acc = acc + arrived[j - 1, row, :].astype(jnp.float32)
        out_ref[:, row] = acc.T.astype(out_ref.dtype)
        return carry

    def total_if(i, carry):
        is_tail = (lax.rem(i * 128, rows) == tail) & (lax.rem(i * 128 // rows, n_fs) == far)

        @pl.when(tail_here | jnp.logical_not(is_tail))
        def _():
            total(i, 0)

        return carry

    lax.fori_loop(0, final_tile, total_if, 0)
    lax.fori_loop(last_tile, depth // 128, total_if, 0)

    if tail > 0:
        settled(arrived.at[:, pl.ds(0, tail), :], part_recv.at[1])
    lax.fori_loop(final_tile, last_tile, total, 0)
    parts_settled(0, part_send.at[0])
    settled(others, tok_sem.at[0])
    if helped:
        pl.when(at_end)(lambda: hidden_copy().wait_send())
        pl.when(helping)(lambda: settled(far_arrived, far_sem.at[0]))

    def sent_blocks(here):
        for p in range(2):
            right = left = across = 0
            for zz in range(n_fs):
                for k, (_, size) in enumerate(tables[p][2]):
                    right += size * (zz <= here and goes(p, zz, k, True, here))
                    left += size * (zz >= here and goes(p, zz, k, False, here))
                    by_x = k in near[p] or (k in rest[p] and rest_by_x(zz, here)) or (k == cross[p] and zz == here)
                    across += size * by_x
            settled_rows(right, right_send.at[p])
            settled_rows(left, left_send.at[p])
            settled_rows(across, x_send.at[p])

    for here in range(n_fs):
        pl.when(z == here)(functools.partial(sent_blocks, here))
    if helped:
        last_in()

        pl.when(at_end)(lambda: settled(far_out, give_sem.at[1]))
        pl.when(helping)(lambda: settled(far_out, give_sem.at[0]))


def write_out(*refs):
    held, outs, sem = refs[:3], refs[3:6], refs[6]
    for i, (src, dst) in enumerate(zip(held, outs)):
        rows = src.shape[0] // WRITES
        for k in range(WRITES):
            part = pl.ds(k * rows, rows)
            pltpu.make_async_copy(src.at[part, :], dst.at[part, :], sem.at[i]).start()
    for i, (src, dst) in enumerate(zip(held, outs)):
        pltpu.make_async_copy(src, dst, sem.at[i]).wait()


def solution(mesh):
    n_gr, n_fs, n_tp = (mesh.shape[a] for a in ("gr", "fs", "tp"))

    def on_device(prompt_tokens, norm_gain, up_master, down_master):
        local, depth = prompt_tokens.shape
        rows, width = up_master.shape
        tables = split_rows(rows)[1]
        most = max(len(table) for _, _, table in tables)
        dma = pltpu.SemaphoreType.DMA
        bf16 = jnp.bfloat16
        anywhere = pl.BlockSpec(memory_space=pl.ANY)
        vmem = pl.BlockSpec(memory_space=pltpu.VMEM)
        held = pl.pallas_call(
            functools.partial(kernel, (n_gr, n_fs, n_tp)),
            out_shape=(
                pltpu.VMEM((depth, width), bf16),
                pltpu.VMEM((depth, width), bf16),
                pltpu.VMEM((local, depth), bf16),
            ),
            in_specs=[anywhere] * 4,
            out_specs=(vmem, vmem, vmem),
            scratch_shapes=[
                pltpu.VMEM((local, depth), bf16),
                pltpu.VMEM((1, rows), jnp.float32),
                pltpu.VMEM((2, rows, width), jnp.float32),
                pltpu.VMEM((local * n_tp, depth), bf16),
                pltpu.VMEM((local * n_tp, width), bf16),
                pltpu.VMEM((depth, local * n_tp), bf16),
                pltpu.VMEM((n_tp - 1, depth, local), bf16),
                pltpu.VMEM((local * n_tp, width), bf16),
                pltpu.VMEM((256, local * n_tp), bf16),
                pltpu.VMEM((n_tp - 1, 256, local), bf16),
                pltpu.VMEM((2, local, 128), bf16),
                dma((3,)), dma((most,)), dma((2,)),
                dma((2, max(1, n_fs - 1), most)), dma((2,)), dma((2,)), dma((3 + 2 * n_fs,)), dma((2,)),
                dma((1,)), dma((2,)), dma((2,)), dma((2,)), dma((2,)),
            ],
            compiler_params=pltpu.CompilerParams(
                collective_id=0, has_side_effects=True, vmem_limit_bytes=44 * 2**20
            ),
        )(norm_gain[None, :], prompt_tokens, up_master, down_master)
        return pl.pallas_call(
            write_out,
            out_shape=(
                jax.ShapeDtypeStruct((depth, width), bf16),
                jax.ShapeDtypeStruct((depth, width), bf16),
                jax.ShapeDtypeStruct((local, depth), bf16),
            ),
            in_specs=[vmem, vmem, vmem],
            out_specs=(anywhere, anywhere, anywhere),
            scratch_shapes=[dma((3,))],
            compiler_params=pltpu.CompilerParams(vmem_limit_bytes=2**20),
        )(*held)

    placed = (
        P(("gr", "fs", "tp"), None),
        P(("gr", "fs")),
        P(("gr", "fs"), "tp"),
        P(("gr", "fs"), "tp"),
    )
    return jax.shard_map(
        on_device,
        mesh=mesh,
        in_specs=placed,
        out_specs=(P(None, "tp"), P(None, "tp"), P(("gr", "fs", "tp"), None)),
        check_vma=False,
    )
```

time: 177 us -> 172 us (0.972)
  Pallas kernels: 176 us -> 171 us
    pallas_call x1, Pallas kernels: 170 us -> 165 us  [on_device(): pl.pallas_call(functools.partial(kernel, (n_gr, n_fs, n_tp)), out_shape=(...]
where the time goes in v3:
time: 172 us; the launch traced here: 171 us
  Pallas kernels  171 us (99%)
    pallas_call x1, Pallas kernels, on_device(): pl.pallas_call(functools.partial(kernel, (n_gr, n_fs, n_tp)), out_shape=(...  165 us
    pallas_call x1, Pallas kernels, on_device(): pl.pallas_call(write_out, out_shape=(jax.ShapeDtypeStruct((depth, width),...  5.96 us

profile of v3, /device:TPU:0, one launch (start us, length us, event | category | flops | bytes accessed | tf_op | source)
XLA Modules:
  0.0 171.5 jit_solution(15510528235938426449)
XLA Ops:
  0.6 164.9 %shard_map.67 = (bf16[2048,2048]{1,0:T(8,128)(2,1)S(1)}, bf16[2048,2048]{1,0:T(8,128)(2,1)S(1)}, bf16[128,2048]{1,0:T(8,128)(2,1)S(1)}) custom-call(f32[1,256]{1,0:T(1,128)} %bitcast.1, bf16[128,2048]{1,0:T(8,128)(2,1)} %tok_hbm.1, f32[256,2048]{1,0:T(8,128)} %up_hbm.1, f32[256,2048]{1,0:T(8,128)} %down_hbm.1), custom_call_target="tpu_custom_call" | custom-call | tf_op jit(solution)/shard_map/pallas_call | solution.py:481
  165.5 6.0 %shard_map.68 = (bf16[2048,2048]{1,0:T(8,128)(2,1)}, bf16[2048,2048]{1,0:T(8,128)(2,1)}, bf16[128,2048]{1,0:T(8,128)(2,1)}) custom-call(bf16[2048,2048]{1,0:T(8,128)(2,1)S(1)} %get-tuple-element.6.refs_0_, bf16[2048,2048]{1,0:T(8,128)(2,1)S(1)} %get-tuple-element.7.refs_1_, bf16[128,2048]{1,0:T(8,128)(2,1)S(1)} %get-tuple-element.8.refs_2_), custom_call_target="tpu_custom_call" | custom-call | tf_op jit(solution)/shard_map/pallas_call | solution.py:510

commit v4 on v3

--- a/solution.py
+++ b/solution.py
@@ -18,13 +18,21 @@
     return [(a, b - a) for a, b in zip(cuts, cuts[1:]) if b > a]
 
 
-def split_rows(rows):
+def split_rows(rows, width):
+    def wide(pieces):
+        return [(start, size, 0, width) for start, size in pieces]
+
     tail = max(0, rows - 128)
     edge = rows - max(8, rows * 5 // 256 * 8)
-    tables = []
-    for cut, pieces in ((edge, PIECES[0]), (min(tail, edge), PIECES[1])):
-        near, rest, cross = pieces_of(0, cut, pieces), pieces_of(cut, edge, PIECES[2]), [(edge, rows - edge)]
-        tables.append((near, rest, near + rest + cross + cross + rest))
+    near, cross = wide(pieces_of(0, edge, PIECES[0])), wide([(edge, rows - edge)])
+    tables = [(near, [], near + cross + cross)]
+    edge = rows - max(8, rows * 6 // 256 * 8)
+    column = width * 7 // 8 // 128 * 128
+    cut = min(tail, edge)
+    near, rest = wide(pieces_of(0, cut, PIECES[1])), wide(pieces_of(cut, edge, PIECES[2]))
+    rest.append((edge, rows - edge, column, width - column))
+    cross = [(edge, rows - edge, 0, column)]
+    tables.append((near, rest, near + rest + cross + cross + rest))
     return tail, tables
 
 
@@ -47,7 +55,7 @@
     at_end = (z == 0) | (z == last)
     masters = (up_ref, down_ref)
 
-    tail, tables = split_rows(rows)
+    tail, tables = split_rows(rows, width)
     helped = n_fs >= 4 and rows % 128 == 0
     near = [range(len(a)) for a, _, _ in tables]
     rest = [range(len(a), len(a) + len(b)) for a, b, _ in tables]
@@ -70,21 +78,30 @@
 
     def settled_rows(count, sem):
         if count:
-            settled(up_ref.at[pl.ds(0, count), :], sem)
+            tiles = count * width // 1024
+            across = next(c for c in range(width // 128, 0, -1) if tiles % c == 0)
+            settled(up_ref.at[pl.ds(0, tiles // across * 8), pl.ds(0, across * 128)], sem)
 
     def size_of(p, items):
-        return sum(tables[p][2][k][1] for k in items)
+        return sum(size * columns for _, size, _, columns in (tables[p][2][k] for k in items)) // width
 
     def at(p, col, zz, k):
-        start, size = tables[p][2][k]
+        start, size, column, columns = tables[p][2][k]
         base = pl.multiple_of((col * n_fs + zz) * rows, rows)
-        return masters[p].at[pl.ds(pl.multiple_of(base + start, 8), size), :]
+        return masters[p].at[pl.ds(pl.multiple_of(base + start, 8), size), pl.ds(column, columns)]
+
+    def kind(p, k):
+        return p if tables[p][2][k][3] == width else 2
+
+    def z_sem(p, zz, k, right):
+        item = (len(tables[0][2]) if p else 0) + min(k, cross[p] + 2)
+        return z_recv.at[zz if right else zz - 1, item]
 
     def z_copy(p, zz, k, right):
         ref = at(p, 1 - g if k > cross[p] else g, zz, k)
         send = right_send if right else left_send
         return pltpu.make_async_remote_copy(
-            src_ref=ref, dst_ref=ref, send_sem=send.at[p], recv_sem=z_recv.at[p, zz if right else zz - 1, k],
+            src_ref=ref, dst_ref=ref, send_sem=send.at[kind(p, k)], recv_sem=z_sem(p, zz, k, right),
             device_id=(g, jnp.where(has_right, z + 1, z - 1) if right else jnp.where(has_left, z - 1, z + 1), t),
             device_id_type=MESH,
         )
@@ -99,7 +116,7 @@
     def x_copy(p, zz, k, col):
         ref = at(p, col, zz, k)
         return pltpu.make_async_remote_copy(
-            src_ref=ref, dst_ref=ref, send_sem=x_send.at[p], recv_sem=x_sem(p, zz, k),
+            src_ref=ref, dst_ref=ref, send_sem=x_send.at[kind(p, k)], recv_sem=x_sem(p, zz, k),
             device_id=(1 - g, z, t), device_id_type=MESH,
         )
 
@@ -135,12 +152,21 @@
     def slot(p, s, items):
         for k in items:
             wide = k in extra[p]
+            if wide and (s == last or k > extra[p][0]):
+                continue
 
             def come(right):
                 zz = z - s if right else z + s
-                z_copy(p, zz, k, right).wait_recv()
+                if wide:
+                    settled_rows(size_of(p, extra[p]), z_sem(p, zz, k, right))
+                else:
+                    z_copy(p, zz, k, right).wait_recv()
                 if s < last:
-                    pl.when(goes(p, zz, k, right, z))(lambda: z_copy(p, zz, k, right).start())
+                    @pl.when(goes(p, zz, k, right, z))
+                    def _():
+                        for item in extra[p] if wide else (k,):
+                            z_copy(p, zz, item, right).start()
+
                 if k in near[p]:
                     x_copy(p, zz, k, g).start()
                 elif k in rest[p]:
@@ -149,9 +175,8 @@
             from_left, from_right = z - s >= 0, z + s <= last
             if wide:
                 from_left, from_right = (z - s == 0) & has_right, (z + s == last) & has_left
-            if not wide or s < last:
-                pl.when(from_left)(lambda: come(True))
-                pl.when(from_right)(lambda: come(False))
+            pl.when(from_left)(lambda: come(True))
+            pl.when(from_right)(lambda: come(False))
 
     def whole_slot(p, s):
         slot(p, s, range(len(tables[p][2])))
@@ -291,7 +316,7 @@
     order = [cross[0], *near[0]]
 
     def up_load(k):
-        start, size = tables[0][2][k]
+        start, size = tables[0][2][k][:2]
         row = pl.ds(start, size)
         return pltpu.make_async_copy(up_hbm.at[row, :], stage.at[0, row, :], up_sem.at[k])
 
@@ -307,7 +332,7 @@
     loads[2].start()
 
     def round_up(k):
-        start, size = tables[0][2][k]
+        start, size = tables[0][2][k][:2]
         row = pl.ds(pl.multiple_of((g * n_fs + z) * rows + start, 8), size)
         up_load(k).wait()
         up_ref[row, :] = (stage[0, start : start + size] * gain[start : start + size]).astype(up_ref.dtype)
@@ -434,17 +459,18 @@
         pl.when(helping)(lambda: settled(far_arrived, far_sem.at[0]))
 
     def sent_blocks(here):
+        sent = [[0, 0, 0] for _ in range(3)]
         for p in range(2):
-            right = left = across = 0
             for zz in range(n_fs):
-                for k, (_, size) in enumerate(tables[p][2]):
-                    right += size * (zz <= here and goes(p, zz, k, True, here))
-                    left += size * (zz >= here and goes(p, zz, k, False, here))
-                    by_x = k in near[p] or (k in rest[p] and rest_by_x(zz, here)) or (k == cross[p] and zz == here)
-                    across += size * by_x
-            settled_rows(right, right_send.at[p])
-            settled_rows(left, left_send.at[p])
-            settled_rows(across, x_send.at[p])
+                for k in range(len(tables[p][2])):
+                    size, to = size_of(p, [k]), kind(p, k)
+                    by_x = k in near[p] or (k in rest[p] and rest_by_x(zz, here)) or (k <= cross[p] and zz == here)
+                    sent[0][to] += size * (zz <= here and goes(p, zz, k, True, here))
+                    sent[1][to] += size * (zz >= here and goes(p, zz, k, False, here))
+                    sent[2][to] += size * by_x
+        for counts, sem in zip(sent, (right_send, left_send, x_send)):
+            for to, count in enumerate(counts):
+                settled_rows(count, sem.at[to])
 
     for here in range(n_fs):
         pl.when(z == here)(functools.partial(sent_blocks, here))
@@ -472,8 +498,7 @@
     def on_device(prompt_tokens, norm_gain, up_master, down_master):
         local, depth = prompt_tokens.shape
         rows, width = up_master.shape
-        tables = split_rows(rows)[1]
-        most = max(len(table) for _, _, table in tables)
+        ups, downs = (len(table) for _, _, table in split_rows(rows, width)[1])
         dma = pltpu.SemaphoreType.DMA
         bf16 = jnp.bfloat16
         anywhere = pl.BlockSpec(memory_space=pl.ANY)
@@ -499,8 +524,8 @@
                 pltpu.VMEM((256, local * n_tp), bf16),
                 pltpu.VMEM((n_tp - 1, 256, local), bf16),
                 pltpu.VMEM((2, local, 128), bf16),
-                dma((3,)), dma((most,)), dma((2,)),
-                dma((2, max(1, n_fs - 1), most)), dma((2,)), dma((2,)), dma((3 + 2 * n_fs,)), dma((2,)),
+                dma((3,)), dma((ups,)), dma((2,)),
+                dma((max(1, n_fs - 1), ups + downs)), dma((3,)), dma((3,)), dma((3 + 2 * n_fs,)), dma((3,)),
                 dma((1,)), dma((2,)), dma((2,)), dma((2,)), dma((2,)),
             ],
             compiler_params=pltpu.CompilerParams(

time: 172 us -> 171 us (level)
  no operation moved by 1% of the time
where the time goes in v4:
time: 171 us
  Pallas kernels  170 us (99%)
    pallas_call x1, Pallas kernels, on_device(): pl.pallas_call(functools.partial(kernel, (n_gr, n_fs, n_tp)), out_shape=(...  164 us
    pallas_call x1, Pallas kernels, on_device(): pl.pallas_call(write_out, out_shape=(jax.ShapeDtypeStruct((depth, width),...  5.96 us

profile of v4, /device:TPU:0, one launch (start us, length us, event | category | flops | bytes accessed | tf_op | source)
XLA Modules:
  0.0 171.0 jit_solution(513766398701378315)
XLA Ops:
  0.6 164.4 %shard_map.67 = (bf16[2048,2048]{1,0:T(8,128)(2,1)S(1)}, bf16[2048,2048]{1,0:T(8,128)(2,1)S(1)}, bf16[128,2048]{1,0:T(8,128)(2,1)S(1)}) custom-call(f32[1,256]{1,0:T(1,128)} %bitcast.1, bf16[128,2048]{1,0:T(8,128)(2,1)} %tok_hbm.1, f32[256,2048]{1,0:T(8,128)} %up_hbm.1, f32[256,2048]{1,0:T(8,128)} %down_hbm.1), custom_call_target="tpu_custom_call" | custom-call | tf_op jit(solution)/shard_map/pallas_call | solution.py:506
  165.1 6.0 %shard_map.68 = (bf16[2048,2048]{1,0:T(8,128)(2,1)}, bf16[2048,2048]{1,0:T(8,128)(2,1)}, bf16[128,2048]{1,0:T(8,128)(2,1)}) custom-call(bf16[2048,2048]{1,0:T(8,128)(2,1)S(1)} %get-tuple-element.6.refs_0_, bf16[2048,2048]{1,0:T(8,128)(2,1)S(1)} %get-tuple-element.7.refs_1_, bf16[128,2048]{1,0:T(8,128)(2,1)S(1)} %get-tuple-element.8.refs_2_), custom_call_target="tpu_custom_call" | custom-call | tf_op jit(solution)/shard_map/pallas_call | solution.py:535

commit v5 on v4

--- a/solution.py
+++ b/solution.py
@@ -10,6 +10,7 @@
 MESH = pl.DeviceIdType.MESH
 PIECES = (3, 2, 1)
 WRITES = 4
+DELAY = 19000
 
 
 def pieces_of(start, stop, count):
@@ -36,24 +37,26 @@
     return tail, tables
 
 
-def kernel(
-    sizes, gain_hbm, tok_hbm, up_hbm, down_hbm,
-    up_ref, down_ref, out_ref,
-    tok_ref, gain_ref, stage, normed, hidden, part, arrived,
-    far_hidden, far_part, far_arrived, far_out,
-    load_sem, up_sem, tok_sem,
-    z_recv, right_send, left_send, x_recv, x_send, part_send, part_recv,
-    hid_sem, far_sem, give_sem,
-):
+def kernel(phase, sizes, *refs):
+    if phase == 0:
+        (gain_hbm, tok_hbm, up_hbm, up_ref, normed, tok_ref, gain_ref, stage, load_sem, up_sem, tok_sem,
+         z_recv, right_send, left_send, x_recv, x_send) = refs
+        master = up_ref
+    else:
+        (up_ref, normed, stage, _, down_ref, out_ref, hidden, part, arrived,
+         far_hidden, far_part, far_arrived, far_out,
+         z_recv, right_send, left_send, x_recv, x_send, part_send, part_recv,
+         hid_sem, far_sem, give_sem, late_sem) = refs
+        master = down_ref
     n_gr, n_fs, n_tp = sizes
     g, z, t = lax.axis_index("gr"), lax.axis_index("fs"), lax.axis_index("tp")
-    rows, width = stage.shape[1:]
-    local = tok_ref.shape[0]
+    rows, width = stage.shape
+    local = normed.shape[0] // n_tp
     depth = up_ref.shape[0]
+    odd = lax.rem(t, 2) == 1
     last = n_fs - 1
     has_right, has_left = z < last, z > 0
     at_end = (z == 0) | (z == last)
-    masters = (up_ref, down_ref)
 
     tail, tables = split_rows(rows, width)
     helped = n_fs >= 4 and rows % 128 == 0
@@ -80,7 +83,7 @@
         if count:
             tiles = count * width // 1024
             across = next(c for c in range(width // 128, 0, -1) if tiles % c == 0)
-            settled(up_ref.at[pl.ds(0, tiles // across * 8), pl.ds(0, across * 128)], sem)
+            settled(master.at[pl.ds(0, tiles // across * 8), pl.ds(0, across * 128)], sem)
 
     def size_of(p, items):
         return sum(size * columns for _, size, _, columns in (tables[p][2][k] for k in items)) // width
@@ -88,14 +91,13 @@
     def at(p, col, zz, k):
         start, size, column, columns = tables[p][2][k]
         base = pl.multiple_of((col * n_fs + zz) * rows, rows)
-        return masters[p].at[pl.ds(pl.multiple_of(base + start, 8), size), pl.ds(column, columns)]
+        return master.at[pl.ds(pl.multiple_of(base + start, 8), size), pl.ds(column, columns)]
 
     def kind(p, k):
-        return p if tables[p][2][k][3] == width else 2
+        return 0 if tables[p][2][k][3] == width else 1
 
     def z_sem(p, zz, k, right):
-        item = (len(tables[0][2]) if p else 0) + min(k, cross[p] + 2)
-        return z_recv.at[zz if right else zz - 1, item]
+        return z_recv.at[zz if right else zz - 1, min(k, cross[p] + 2)]
 
     def z_copy(p, zz, k, right):
         ref = at(p, 1 - g if k > cross[p] else g, zz, k)
@@ -108,10 +110,10 @@
 
     def x_sem(p, zz, k):
         if k == cross[p]:
-            return x_recv.at[p]
+            return x_recv.at[0]
         if p == 0:
-            return x_recv.at[2]
-        return x_recv.at[3 + zz + (0 if k in near[1] else n_fs)]
+            return x_recv.at[1]
+        return x_recv.at[1 + zz + (0 if k in near[1] else n_fs)]
 
     def x_copy(p, zz, k, col):
         ref = at(p, col, zz, k)
@@ -137,10 +139,10 @@
         send_both(p, cross[p] + 1)
 
     def near_in(zz):
-        settled_rows(size_of(1, near[1]), x_recv.at[3 + zz])
+        settled_rows(size_of(1, near[1]), x_recv.at[1 + zz])
 
     def rest_in(zz):
-        settled_rows(size_of(1, rest[1]), x_recv.at[3 + n_fs + zz])
+        settled_rows(size_of(1, rest[1]), x_recv.at[1 + n_fs + zz])
 
     def other_rest(p):
         @pl.when(at_end)
@@ -302,6 +304,23 @@
         pl.when(at_end)(lambda: settled(arrived.at[:, pl.ds(0, every - 256), :], sem))
         pl.when(tail_here)(lambda: settled(arrived.at[:, pl.ds(0, every), :], sem))
 
+    def sent_blocks(p, here):
+        sent = [[0, 0] for _ in range(3)]
+        for zz in range(n_fs):
+            for k in range(len(tables[p][2])):
+                size, to = size_of(p, [k]), kind(p, k)
+                by_x = k in near[p] or (k in rest[p] and rest_by_x(zz, here)) or (k <= cross[p] and zz == here)
+                sent[0][to] += size * (zz <= here and goes(p, zz, k, True, here))
+                sent[1][to] += size * (zz >= here and goes(p, zz, k, False, here))
+                sent[2][to] += size * by_x
+        for counts, sem in zip(sent, (right_send, left_send, x_send)):
+            for to, count in enumerate(counts):
+                settled_rows(count, sem.at[to])
+
+    def all_sent(p):
+        for here in range(n_fs):
+            pl.when(z == here)(functools.partial(sent_blocks, p, here))
+
     barrier = pltpu.get_barrier_semaphore()
 
     def greet(device):
@@ -311,183 +330,184 @@
     pl.when(has_right)(lambda: greet((g, z + 1, t)))
     pl.when(has_left)(lambda: greet((g, z - 1, t)))
     for j in range(1, n_tp):
-        greet((g, z, lax.rem(t + j, n_tp)))
-
-    order = [cross[0], *near[0]]
-
-    def up_load(k):
-        start, size = tables[0][2][k][:2]
-        row = pl.ds(start, size)
-        return pltpu.make_async_copy(up_hbm.at[row, :], stage.at[0, row, :], up_sem.at[k])
-
-    loads = [
-        pltpu.make_async_copy(gain_hbm, gain_ref, load_sem.at[0]),
-        pltpu.make_async_copy(tok_hbm, tok_ref, load_sem.at[1]),
-        pltpu.make_async_copy(down_hbm, stage.at[1], load_sem.at[2]),
-    ]
-    loads[0].start()
-    for k in order:
-        up_load(k).start()
-    loads[1].start()
-    loads[2].start()
-
-    def round_up(k):
-        start, size = tables[0][2][k][:2]
-        row = pl.ds(pl.multiple_of((g * n_fs + z) * rows + start, 8), size)
-        up_load(k).wait()
-        up_ref[row, :] = (stage[0, start : start + size] * gain[start : start + size]).astype(up_ref.dtype)
-
-    def send_own(k):
-        x_copy(0, z, k, g).start()
-        if k != cross[0]:
-            send_both(0, k)
-
-    own = pl.ds(pl.multiple_of((g * n_fs + z) * rows, rows), rows)
-    square = (rows, rows)
-    on_diagonal = lax.broadcasted_iota(jnp.int32, square, 0) == lax.broadcasted_iota(jnp.int32, square, 1)
-    loads[0].wait()
-    gain = jnp.sum(jnp.where(on_diagonal, gain_ref[...], 0.0), axis=1, keepdims=True)
-    round_up(order[0])
-    round_up(order[1])
-    pl.semaphore_wait(barrier, n_tp + has_right.astype(jnp.int32) + has_left.astype(jnp.int32))
-    for i, k in enumerate(order):
-        send_own(k)
-        if i + 2 < len(order):
-            round_up(order[i + 2])
-    send_both(0, cross[0])
-
-    loads[1].wait()
-    floats = tok_ref[...].astype(jnp.float32)
-    mean_square = jnp.mean(floats * floats, axis=1, keepdims=True)
-    normed[pl.ds(pl.multiple_of(t * local, local), local), :] = (
-        floats * lax.rsqrt(mean_square + 1e-06)
-    ).astype(normed.dtype)
-    for j in range(1, n_tp):
-        token_copy(j).start()
-    other_xz(0)
-    loads[2].wait()
-    down_ref[own, :] = stage[1].astype(down_ref.dtype)
-
-    for s in range(1, last):
-        whole_slot(0, s)
-    own_z(1)
-    if last > 0:
-        slot(0, last, near[0])
-    own_x(1)
-    if last > 0:
-        slot(0, last, range(cross[0], cross[0] + 2))
-
-    settled_rows(n_fs * size_of(0, near[0]), x_recv.at[2])
-    others = normed.at[pl.ds(0, (n_tp - 1) * local), :]
-    settled(others, tok_sem.at[1])
-
-    tile = 256
-
-    def first(i, carry):
-        columns = pl.ds(pl.multiple_of(i * tile, tile), tile)
-        pre = jnp.dot(normed[...], up_ref[:, columns], preferred_element_type=jnp.float32)
-        hidden[:, columns] = jnp.square(jnp.maximum(pre, 0.0)).astype(hidden.dtype)
-        return carry
-
-    lax.fori_loop(0, width // tile, first, 0)
-
-    other_xz(1)
-    other_rest(1)
-    if helped:
-        @pl.when(at_end)
+        if phase == 0 or j % 2 == 0:
+            greet((g, z, lax.rem(t + j, n_tp)))
+        else:
+            pl.when(jnp.logical_not(odd))(functools.partial(greet, (g, z, lax.rem(t + j, n_tp))))
+
+    def gather_up():
+        order = [cross[0], *near[0]]
+
+        def up_load(k):
+            start, size = tables[0][2][k][:2]
+            row = pl.ds(start, size)
+            return pltpu.make_async_copy(up_hbm.at[row, :], stage.at[row, :], up_sem.at[k])
+
+        loads = [
+            pltpu.make_async_copy(gain_hbm, gain_ref, load_sem.at[0]),
+            pltpu.make_async_copy(tok_hbm, tok_ref, load_sem.at[1]),
+        ]
+        loads[0].start()
+        for k in order:
+            up_load(k).start()
+        loads[1].start()
+
+        def round_up(k):
+            start, size = tables[0][2][k][:2]
+            row = pl.ds(pl.multiple_of((g * n_fs + z) * rows + start, 8), size)
+            up_load(k).wait()
+            up_ref[row, :] = (stage[start : start + size] * gain[start : start + size]).astype(up_ref.dtype)
+
+        def send_own(k):
+            x_copy(0, z, k, g).start()
+            if k != cross[0]:
+                send_both(0, k)
+
+        square = (rows, rows)
+        on_diagonal = lax.broadcasted_iota(jnp.int32, square, 0) == lax.broadcasted_iota(jnp.int32, square, 1)
+        loads[0].wait()
+        gain = jnp.sum(jnp.where(on_diagonal, gain_ref[...], 0.0), axis=1, keepdims=True)
+        round_up(order[0])
+        round_up(order[1])
+        pl.semaphore_wait(barrier, n_tp + has_right.astype(jnp.int32) + has_left.astype(jnp.int32))
+        pl.when(odd)(lambda: pl.delay(DELAY))
+        for i, k in enumerate(order):
+            send_own(k)
+            if i + 2 < len(order):
+                round_up(order[i + 2])
+        send_both(0, cross[0])
+
+        loads[1].wait()
+        floats = tok_ref[...].astype(jnp.float32)
+        mean_square = jnp.mean(floats * floats, axis=1, keepdims=True)
+        normed[pl.ds(pl.multiple_of(t * local, local), local), :] = (
+            floats * lax.rsqrt(mean_square + 1e-06)
+        ).astype(normed.dtype)
+        for j in range(1, n_tp):
+            token_copy(j).start()
+        other_xz(0)
+
+        for s in range(1, last + 1):
+            whole_slot(0, s)
+        settled_rows(n_fs * size_of(0, near[0]), x_recv.at[1])
+        others = normed.at[pl.ds(0, (n_tp - 1) * local), :]
+        settled(others, tok_sem.at[1])
+        settled(others, tok_sem.at[0])
+        all_sent(0)
+
+    def gather_down():
+        def late(device):
+            pl.semaphore_signal(late_sem, inc=1, device_id=device, device_id_type=MESH)
+
+        own = pl.ds(pl.multiple_of((g * n_fs + z) * rows, rows), rows)
+        down_ref[own, :] = stage[...].astype(down_ref.dtype)
+        sides = has_right.astype(jnp.int32) + has_left.astype(jnp.int32)
+        pl.semaphore_wait(barrier, n_tp // 2 + sides + odd.astype(jnp.int32) * (n_tp // 2))
+        own_z(1)
+        own_x(1)
+
+        @pl.when(odd)
         def _():
-            hidden_copy().start()
-
-    second(0)
-    for s in range(1, last):
-        whole_slot(1, s)
-        second(s)
-    slot(1, last, near[1])
-    second(last)
-    far_share(g, 0)
-    slot(1, last, rest[1])
-    if helped:
-        pl.when(tail_here)(far_tails)
-        pl.when(helping)(help_multiply)
-    near_in(far)
-    far_share(1 - g, 0, True)
-    if helped:
-        pl.when(helping)(help_total)
-
-    def last_in():
-        slot(1, last, range(cross[1], cross[1] + 2))
-
-        pl.when(at_end)(lambda: rest_in(far))
-
-    if not helped:
-        last_in()
-        far_tails()
-
-    final = (1 - g) * n_fs + far
-    final_tile = final * (rows // 128)
-    last_tile = final_tile + tail // 128
-
-    parts_settled(tail, part_recv.at[0])
-
-    def total(i, carry):
-        row = pl.ds(pl.multiple_of(i * 128, 128), 128)
-        acc = part[row, pl.ds(pl.multiple_of(t * local, local), local)].astype(jnp.float32)
-        for j in range(1, n_tp):
-            acc = acc + arrived[j - 1, row, :].astype(jnp.float32)
-        out_ref[:, row] = acc.T.astype(out_ref.dtype)
-        return carry
-
-    def total_if(i, carry):
-        is_tail = (lax.rem(i * 128, rows) == tail) & (lax.rem(i * 128 // rows, n_fs) == far)
-
-        @pl.when(tail_here | jnp.logical_not(is_tail))
-        def _():
-            total(i, 0)
-
-        return carry
-
-    lax.fori_loop(0, final_tile, total_if, 0)
-    lax.fori_loop(last_tile, depth // 128, total_if, 0)
-
-    if tail > 0:
-        settled(arrived.at[:, pl.ds(0, tail), :], part_recv.at[1])
-    lax.fori_loop(final_tile, last_tile, total, 0)
-    parts_settled(0, part_send.at[0])
-    settled(others, tok_sem.at[0])
-    if helped:
-        pl.when(at_end)(lambda: hidden_copy().wait_send())
-        pl.when(helping)(lambda: settled(far_arrived, far_sem.at[0]))
-
-    def sent_blocks(here):
-        sent = [[0, 0, 0] for _ in range(3)]
-        for p in range(2):
-            for zz in range(n_fs):
-                for k in range(len(tables[p][2])):
-                    size, to = size_of(p, [k]), kind(p, k)
-                    by_x = k in near[p] or (k in rest[p] and rest_by_x(zz, here)) or (k <= cross[p] and zz == here)
-                    sent[0][to] += size * (zz <= here and goes(p, zz, k, True, here))
-                    sent[1][to] += size * (zz >= here and goes(p, zz, k, False, here))
-                    sent[2][to] += size * by_x
-        for counts, sem in zip(sent, (right_send, left_send, x_send)):
-            for to, count in enumerate(counts):
-                settled_rows(count, sem.at[to])
-
-    for here in range(n_fs):
-        pl.when(z == here)(functools.partial(sent_blocks, here))
-    if helped:
-        last_in()
-
-        pl.when(at_end)(lambda: settled(far_out, give_sem.at[1]))
-        pl.when(helping)(lambda: settled(far_out, give_sem.at[0]))
-
-
-def write_out(*refs):
-    held, outs, sem = refs[:3], refs[3:6], refs[6]
+            for j in range(1, n_tp, 2):
+                late((g, z, lax.rem(t + j, n_tp)))
+
+        tile = 256
+
+        def first(i, carry):
+            columns = pl.ds(pl.multiple_of(i * tile, tile), tile)
+            pre = jnp.dot(normed[...], up_ref[:, columns], preferred_element_type=jnp.float32)
+            hidden[:, columns] = jnp.square(jnp.maximum(pre, 0.0)).astype(hidden.dtype)
+            return carry
+
+        lax.fori_loop(0, width // tile, first, 0)
+        wait_late = lambda: pl.semaphore_wait(late_sem, n_tp // 2)
+        other_xz(1)
+        other_rest(1)
+        if helped:
+            @pl.when(at_end)
+            def _():
+                hidden_copy().start()
+
+        for s in range(1, last):
+            whole_slot(1, s)
+            if s == 1:
+                pl.when(jnp.logical_not(odd))(wait_late)
+                second(0)
+            second(s)
+        slot(1, last, near[1])
+        second(last)
+        far_share(g, 0)
+        slot(1, last, rest[1])
+        if helped:
+            pl.when(tail_here)(far_tails)
+            pl.when(helping)(help_multiply)
+        near_in(far)
+        far_share(1 - g, 0, True)
+        if helped:
+            pl.when(helping)(help_total)
+
+        def last_in():
+            slot(1, last, range(cross[1], cross[1] + 2))
+
+            pl.when(at_end)(lambda: rest_in(far))
+
+        if not helped:
+            last_in()
+            far_tails()
+
+        final = (1 - g) * n_fs + far
+        final_tile = final * (rows // 128)
+        last_tile = final_tile + tail // 128
+
+        parts_settled(tail, part_recv.at[0])
+
+        def total(i, carry):
+            row = pl.ds(pl.multiple_of(i * 128, 128), 128)
+            acc = part[row, pl.ds(pl.multiple_of(t * local, local), local)].astype(jnp.float32)
+            for j in range(1, n_tp):
+                acc = acc + arrived[j - 1, row, :].astype(jnp.float32)
+            out_ref[:, row] = acc.T.astype(out_ref.dtype)
+            return carry
+
+        def total_if(i, carry):
+            is_tail = (lax.rem(i * 128, rows) == tail) & (lax.rem(i * 128 // rows, n_fs) == far)
+
+            @pl.when(tail_here | jnp.logical_not(is_tail))
+            def _():
+                total(i, 0)
+
+            return carry
+
+        lax.fori_loop(0, final_tile, total_if, 0)
+        lax.fori_loop(last_tile, depth // 128, total_if, 0)
+
+        if tail > 0:
+            settled(arrived.at[:, pl.ds(0, tail), :], part_recv.at[1])
+        lax.fori_loop(final_tile, last_tile, total, 0)
+        parts_settled(0, part_send.at[0])
+        if helped:
+            pl.when(at_end)(lambda: hidden_copy().wait_send())
+            pl.when(helping)(lambda: settled(far_arrived, far_sem.at[0]))
+
+        all_sent(1)
+        if helped:
+            last_in()
+
+            pl.when(at_end)(lambda: settled(far_out, give_sem.at[1]))
+            pl.when(helping)(lambda: settled(far_out, give_sem.at[0]))
+
+    gather_up() if phase == 0 else gather_down()
+
+
+def write_out(count, *refs):
+    held, outs, sem = refs[:count], refs[count : 2 * count], refs[-1]
     for i, (src, dst) in enumerate(zip(held, outs)):
         rows = src.shape[0] // WRITES
         for k in range(WRITES):
             part = pl.ds(k * rows, rows)
             pltpu.make_async_copy(src.at[part, :], dst.at[part, :], sem.at[i]).start()
+    if len(refs) > 2 * count + 1:
+        refs[2 * count][...] = jnp.zeros_like(refs[2 * count])
     for i, (src, dst) in enumerate(zip(held, outs)):
         pltpu.make_async_copy(src, dst, sem.at[i]).wait()
 
@@ -503,20 +523,45 @@
         bf16 = jnp.bfloat16
         anywhere = pl.BlockSpec(memory_space=pl.ANY)
         vmem = pl.BlockSpec(memory_space=pltpu.VMEM)
-        held = pl.pallas_call(
-            functools.partial(kernel, (n_gr, n_fs, n_tp)),
-            out_shape=(
-                pltpu.VMEM((depth, width), bf16),
-                pltpu.VMEM((depth, width), bf16),
-                pltpu.VMEM((local, depth), bf16),
-            ),
-            in_specs=[anywhere] * 4,
-            out_specs=(vmem, vmem, vmem),
+        main = pl.BlockSpec(memory_space=pltpu.HBM)
+        sends = [dma((2,)), dma((2,))]
+
+        weights, tokens, third = depth * width * 2, local * n_tp * depth * 2, local * n_tp * width * 2
+        limits = (64 * 2**20 - weights - tokens - 2**18, 2 * third + rows * width * 4 + 3 * tokens + 8 * 2**20)
+
+        def remote(phase):
+            return pltpu.CompilerParams(collective_id=phase, has_side_effects=True, vmem_limit_bytes=limits[phase])
+
+        kept = functools.partial(pltpu.with_memory_space_constraint, memory_space=pltpu.VMEM)
+        small = pltpu.CompilerParams(vmem_limit_bytes=2**20)
+        up, normed = pl.pallas_call(
+            functools.partial(kernel, 0, (n_gr, n_fs, n_tp)),
+            out_shape=(pltpu.VMEM((depth, width), bf16), pltpu.VMEM((local * n_tp, depth), bf16)),
+            in_specs=[main] * 3,
+            out_specs=(vmem, vmem),
             scratch_shapes=[
                 pltpu.VMEM((local, depth), bf16),
                 pltpu.VMEM((1, rows), jnp.float32),
-                pltpu.VMEM((2, rows, width), jnp.float32),
-                pltpu.VMEM((local * n_tp, depth), bf16),
+                pltpu.VMEM((rows, width), jnp.float32),
+                dma((2,)), dma((ups,)), dma((2,)),
+                dma((max(1, n_fs - 1), ups)), *sends, dma((2,)), dma((2,)),
+            ],
+            compiler_params=remote(0),
+        )(norm_gain[None, :], prompt_tokens, up_master)
+        up_served, after = pl.pallas_call(
+            functools.partial(write_out, 1),
+            out_shape=(jax.ShapeDtypeStruct((depth, width), bf16), pltpu.VMEM((8, 128), jnp.float32)),
+            in_specs=[vmem],
+            out_specs=(anywhere, vmem),
+            scratch_shapes=[dma((1,))],
+            compiler_params=small,
+        )(up)
+        down, out = pl.pallas_call(
+            functools.partial(kernel, 1, (n_gr, n_fs, n_tp)),
+            out_shape=(pltpu.VMEM((depth, width), bf16), pltpu.VMEM((local, depth), bf16)),
+            in_specs=[vmem] * 4,
+            out_specs=(vmem, vmem),
+            scratch_shapes=[
                 pltpu.VMEM((local * n_tp, width), bf16),
                 pltpu.VMEM((depth, local * n_tp), bf16),
                 pltpu.VMEM((n_tp - 1, depth, local), bf16),
@@ -524,26 +569,20 @@
                 pltpu.VMEM((256, local * n_tp), bf16),
                 pltpu.VMEM((n_tp - 1, 256, local), bf16),
                 pltpu.VMEM((2, local, 128), bf16),
-                dma((3,)), dma((ups,)), dma((2,)),
-                dma((max(1, n_fs - 1), ups + downs)), dma((3,)), dma((3,)), dma((3 + 2 * n_fs,)), dma((3,)),
-                dma((1,)), dma((2,)), dma((2,)), dma((2,)), dma((2,)),
+                dma((max(1, n_fs - 1), downs)), *sends, dma((1 + 2 * n_fs,)), dma((2,)),
+                dma((1,)), dma((2,)), dma((2,)), dma((2,)), dma((2,)), pltpu.SemaphoreType.REGULAR,
             ],
-            compiler_params=pltpu.CompilerParams(
-                collective_id=0, has_side_effects=True, vmem_limit_bytes=44 * 2**20
-            ),
-        )(norm_gain[None, :], prompt_tokens, up_master, down_master)
-        return pl.pallas_call(
-            write_out,
-            out_shape=(
-                jax.ShapeDtypeStruct((depth, width), bf16),
-                jax.ShapeDtypeStruct((depth, width), bf16),
-                jax.ShapeDtypeStruct((local, depth), bf16),
-            ),
-            in_specs=[vmem, vmem, vmem],
-            out_specs=(anywhere, anywhere, anywhere),
-            scratch_shapes=[dma((3,))],
-            compiler_params=pltpu.CompilerParams(vmem_limit_bytes=2**20),
-        )(*held)
+            compiler_params=remote(1),
+        )(kept(up), kept(normed), down_master, after)
+        down_served, mlp_output = pl.pallas_call(
+            functools.partial(write_out, 2),
+            out_shape=(jax.ShapeDtypeStruct((depth, width), bf16), jax.ShapeDtypeStruct((local, depth), bf16)),
+            in_specs=[vmem, vmem],
+            out_specs=(anywhere, anywhere),
+            scratch_shapes=[dma((2,))],
+            compiler_params=small,
+        )(down, out)
+        return up_served, down_served, mlp_output
 
     placed = (
         P(("gr", "fs", "tp"), None),

time: 171 us -> 169 us (0.988)
  Pallas kernels: 170 us -> 168 us
    pallas_call x2 -> x4, Pallas kernels: 170 us -> 168 us  [the longest x1 92.6 us: on_device(): pl.pallas_call(functools.partial(kernel, 1, (n_gr, n_fs, n_tp)), out_shap...]
where the time goes in v5:
time: 169 us
  Pallas kernels  168 us (99%)
    pallas_call x1, Pallas kernels, on_device(): pl.pallas_call(functools.partial(kernel, 1, (n_gr, n_fs, n_tp)), out_shap...  92.6 us
    pallas_call x1, Pallas kernels, on_device(): pl.pallas_call(functools.partial(kernel, 0, (n_gr, n_fs, n_tp)), out_shap...  68.4 us
    pallas_call x1, Pallas kernels, on_device(): pl.pallas_call(functools.partial(write_out, 2), out_shape=(jax.ShapeDtype...  3.43 us
    pallas_call x1, Pallas kernels, on_device(): pl.pallas_call(functools.partial(write_out, 1), out_shape=(jax.ShapeDtype...  3.41 us

profile of v5, /device:TPU:0, one launch (start us, length us, event | category | flops | bytes accessed | tf_op | source)
XLA Modules:
  0.0 168.6 jit_solution(17552411466840754229)
XLA Ops:
  0.6 68.4 %shard_map.67 = (bf16[2048,2048]{1,0:T(8,128)(2,1)S(1)}, bf16[512,2048]{1,0:T(8,128)(2,1)S(1)}) custom-call(f32[1,256]{1,0:T(1,128)} %bitcast.1, bf16[128,2048]{1,0:T(8,128)(2,1)} %refs_1_.1, f32[256,2048]{1,0:T(8,128)} %refs_2_.2), custom_call_target="tpu_custom_call" | custom-call | tf_op jit(solution)/shard_map/pallas_call | solution.py:537
  69.1 0.0 copy-start
  69.1 3.4 %shard_map.68 = (bf16[2048,2048]{1,0:T(8,128)(2,1)}, f32[8,128]{1,0:T(8,128)S(1)}) custom-call(bf16[2048,2048]{1,0:T(8,128)(2,1)S(1)} %get-tuple-element.11.refs_0_), custom_call_target="tpu_custom_call" | custom-call | tf_op jit(solution)/shard_map/pallas_call | solution.py:551
  72.5 0.0 copy-done
  72.5 92.6 %shard_map.69 = (bf16[2048,2048]{1,0:T(8,128)(2,1)S(1)}, bf16[128,2048]{1,0:T(8,128)(2,1)S(1)}) custom-call(bf16[2048,2048]{1,0:T(8,128)(2,1)S(1)} %get-tuple-element.11.refs_0_, bf16[512,2048]{1,0:T(8,128)(2,1)S(1)} %get-tuple-element.13.refs_1_, f32[256,2048]{1,0:T(8,128)S(1)} %copy-done, f32[8,128]{1,0:T(8,128)S(1)} %get-tuple-element.14.refs_3_), custom_call_target="tpu_custom_call" | custom-call | tf_op jit(solution)/shard_map/pallas_call | solution.py:559
  165.2 3.4 %shard_map.70 = (bf16[2048,2048]{1,0:T(8,128)(2,1)}, bf16[128,2048]{1,0:T(8,128)(2,1)}) custom-call(bf16[2048,2048]{1,0:T(8,128)(2,1)S(1)} %get-tuple-element.15.refs_0_, bf16[128,2048]{1,0:T(8,128)(2,1)S(1)} %get-tuple-element.16.refs_1_), custom_call_target="tpu_custom_call" | custom-call | tf_op jit(solution)/shard_map/pallas_call | solution.py:577
Async XLA Ops:
  69.1 3.4 %copy-start = (f32[256,2048]{1,0:T(8,128)S(1)}, f32[256,2048]{1,0:T(8,128)}, u32[]{:S(2)}) copy-start(f32[256,2048]{1,0:T(8,128)} %refs_2_.3) | copy-start | bytes 6291460
